TPU v7x, 32 devices: a whole 2x2x4 slice. The times are simulated.
32 devices in a mesh: gr: 2 (over x), sp: 8 (over z, y), tp: 2 (over core).
Axes of the slice: x: 2, y: 2, z: 4, core: 2. Of those that a mesh axis runs over, the one named last changes fastest.
Arguments:
- prompt_elements: bfloat16 [4, 2048, 2048], P('gr', 'sp'), may hold values from -6 to 6
- address_weights: bfloat16 [2048, 1024], P(None, 'tp'), may hold values from -0.125 to 0.125
- content_weights: bfloat16 [2048, 1024], P(None, 'tp'), may hold values from -0.125 to 0.125
- lookup_weights: bfloat16 [2048, 1024], P(None, 'tp'), may hold values from -0.125 to 0.125
- forgetting_weights: bfloat16 [2048, 8], replicated, may hold values from -0.125 to 0.125
- update_intensity_weights: bfloat16 [2048, 8], replicated, may hold values from -0.125 to 0.125
- forgetting_speeds: float32 [8], P('tp'), may hold values from 4.8828125e-05 to 0.05, as said below
- update_intensity_ceiling: float32 [8], P('tp'), may hold values from 0.03125 to 0.125, as said below
- forgetting_multiplier: float32 [4, 2048, 8], P('gr', 'sp', 'tp'), may hold values from 0.35 to 2.8, as said below
- spike_offsets: float32 [4, 2048, 8], P('gr', 'sp', 'tp'), may hold values from -0.7 to 0, as said below
- upcoming_element_vector: bfloat16 [4, 2048], P('gr'), may hold values from -6 to 6
- retrieval_rms_multiplier: float32 [128], replicated, may hold values from 0.1 to 1.9
Outputs:
- cache: bfloat16 [4, 8, 128, 128], P('gr', 'tp', 'sp')
- read: bfloat16 [4, 1024], P('gr', 'tp')
Inputs may be any that keep to these rules, and one draw needn't show every extreme that they name: `forgetting_speeds`: per-head rates of decay. `update_intensity_ceiling`: per-head strength scales. `forgetting_multiplier`: positive factors. `spike_offsets`: non-positive log factors.
All inputs are finite; a program needn't handle non-finite values.
Results may differ from a plain program's by a relative error of at most 0.0037.
Values sent between devices are 32-bit elements; how exact they have to be, the bound alone decides.
No kernel may reach another device: no remote copies, remote signals or barrier semaphores. Data moves between devices by JAX's collectives and lax.ppermute only.
A program may use at most 64 MiB of HBM per device.

v0:
```python
import jax
import jax.numpy as jnp
from jax import lax
from jax.experimental import pallas as pl
from jax.experimental.pallas import tpu as pltpu
from jax.sharding import PartitionSpec as P

EPS = 1e-06
CHUNK = 128
PAD = 8
F32 = jnp.float32
BF16 = jnp.bfloat16
WHOLE = pl.BlockSpec(memory_space=pltpu.VMEM)
SCALARS = pl.BlockSpec(memory_space=pltpu.SMEM)


def dot(a, b):
    return jnp.dot(a, b, preferred_element_type=F32)


def dot_nt(a, b):
    return lax.dot_general(a, b, (((1,), (1,)), ((), ())), preferred_element_type=F32)


def dot_tn(a, b):
    return lax.dot_general(a, b, (((0,), (0,)), ((), ())), preferred_element_type=F32)


def halves(a):
    high = a.astype(BF16)
    return high, (a - high.astype(F32)).astype(BF16)


def dot3(a, b):
    ah, al = halves(a)
    bh, bl = halves(b)
    return dot(ah, bh) + dot(ah, bl) + dot(al, bh)


def silu(values):
    return values * jax.nn.sigmoid(values)


def unit(values):
    return values * lax.rsqrt(jnp.sum(values * values, axis=-1, keepdims=True) + EPS)


def softplus(values):
    return jnp.maximum(values, 0.0) + jnp.log1p(jnp.exp(-jnp.abs(values)))


def pick_lane(values, lane):
    places = lax.broadcasted_iota(jnp.int32, values.shape, 1)
    return jnp.sum(jnp.where(places == lane, values, 0.0), axis=1, keepdims=True)


def chunk_terms(keys, values, strength, cumulative, cumulative_row):
    size = keys.shape[0]
    row = lax.broadcasted_iota(jnp.int32, (size, size), 0)
    col = lax.broadcasted_iota(jnp.int32, (size, size), 1)
    strict = row > col
    short = keys.astype(BF16)
    gram = dot_nt(short, short)
    spread = jnp.exp(jnp.minimum(cumulative - cumulative_row, 0.0))
    lower = jnp.where(strict, gram * strength * spread, 0.0)

    def level(m):
        return (row // (2 * m) == col // (2 * m)) & (row // m != col // m)

    inverse = jnp.where(row == col, 1.0, 0.0) - jnp.where(level(1), lower, 0.0)
    m = 2
    while m < size:
        block = jnp.where(level(m), lower, 0.0).astype(BF16)
        held = inverse.astype(BF16)
        if m < 16:
            inverse = inverse - dot(dot(held, block).astype(BF16), held)
        else:
            odd = [slice(i, i + m) for i in range(m, size, 2 * m)]
            picked = jnp.concatenate([held[s] for s in odd], axis=0)
            change = dot(dot(picked, block).astype(BF16), held)
            parts = []
            for i in range(len(odd)):
                parts.append(inverse[i * 2 * m : i * 2 * m + m])
                parts.append(inverse[odd[i]] - change[i * m : i * m + m])
            inverse = jnp.concatenate(parts, axis=0)
        m *= 2
    off = jnp.where(strict, inverse, 0.0).astype(BF16)
    grown = jnp.exp(cumulative)
    source = jnp.concatenate([keys * (strength * grown), values * strength], axis=1)
    solved = source + dot(off, source.astype(BF16))
    last = cumulative[size - 1 : size]
    faded = (keys * jnp.exp(last - cumulative)).astype(BF16)
    both = dot_tn(faded, solved.astype(BF16))
    width = keys.shape[1]
    return both[:, :width], both[:, width:], jnp.exp(last)


def local_maps_kernel(
    x_ref, wk_ref, wv_ref, wd_ref, ws_ref, speed_ref, ceil_ref, mult_ref, spike_ref,
    keep_ref, send_ref, beta_s, cum_s, row_s,
):
    head = pl.program_id(0)
    seqs, span, width = x_ref.shape
    heads = speed_ref.shape[1]
    dim = wk_ref.shape[1]
    count = seqs * span
    chunks = count // CHUNK
    flat = x_ref[...].reshape(count, width)

    @pl.when(head == 0)
    def _():
        shard = lax.axis_index("tp")

        def mine(full):
            part = full[:, :heads]
            for t in range(1, full.shape[1] // heads):
                part = jnp.where(shard == t, full[:, t * heads : (t + 1) * heads], part)
            return part

        decay_pre = mine(dot(flat, wd_ref[...]))
        strength_pre = mine(dot(flat, ws_ref[...]))
        rate = -speed_ref[...] * softplus(decay_pre)
        gates = rate * mult_ref[...].reshape(count, heads) + spike_ref[...].reshape(count, heads)
        beta_s[:, :heads] = ceil_ref[...] * jax.nn.sigmoid(strength_pre)
        row = lax.broadcasted_iota(jnp.int32, (CHUNK, CHUNK), 0)
        col = lax.broadcasted_iota(jnp.int32, (CHUNK, CHUNK), 1)
        ones = jnp.where(row >= col, 1.0, 0.0)
        for c in range(chunks):
            rows = slice(c * CHUNK, (c + 1) * CHUNK)
            cum_s[rows, :heads] = jnp.dot(
                ones, gates[rows], precision=lax.Precision.HIGHEST, preferred_element_type=F32
            )
            row_s[c] = cum_s[rows, :].T

    weights = jnp.concatenate([wk_ref[...], wv_ref[...]], axis=1)
    raw = dot(flat, weights).astype(BF16).astype(F32)
    keys = unit(silu(raw[:, :dim]))
    values = silu(raw[:, dim:])
    strength = pick_lane(beta_s[...], head)
    cumulative = pick_lane(cum_s[...], head)
    terms = []
    for c in range(chunks):
        rows = slice(c * CHUNK, (c + 1) * CHUNK)
        terms.append(
            chunk_terms(
                keys[rows], values[rows], strength[rows], cumulative[rows],
                row_s[c, pl.ds(head, 1), :],
            )
        )
    row = lax.broadcasted_iota(jnp.int32, (dim, dim), 0)
    col = lax.broadcasted_iota(jnp.int32, (dim, dim), 1)
    eye = jnp.where(row == col, 1.0, 0.0)
    maps = []
    for s in range(seqs):
        mine = terms[s * (chunks // seqs) : (s + 1) * (chunks // seqs)]
        eraser, target, decay = mine[0]
        held_a, held_b = decay * eye - eraser, target
        for eraser, target, decay in mine[1:]:
            both = dot(eraser.astype(BF16), jnp.concatenate([held_a, held_b], axis=1).astype(BF16))
            held_a = decay * held_a - both[:, :dim]
            held_b = decay * held_b - both[:, dim:] + target
        maps.append((held_a, held_b))
    bit = lax.axis_index("sp") % 2
    half = seqs // 2
    for s in range(half):
        for part in range(2):
            first, second = maps[s][part], maps[s + half][part]
            rows = slice(part * dim, (part + 1) * dim)
            keep_ref[s, 0, rows, :] = jnp.where(bit == 0, first, second)
            send_ref[s, 0, rows, :] = jnp.where(bit == 0, second, first)


def local_maps(x, wk, wv, wd, ws, speeds, ceilings, mult, spikes, dim):
    seqs, span, width = x.shape
    heads = speeds.shape[0]
    count = seqs * span
    constant = lambda *shape: pl.BlockSpec(shape, lambda h: (0,) * len(shape))
    column = pl.BlockSpec((width, dim), lambda h: (0, h))
    result = jax.ShapeDtypeStruct((seqs // 2, heads, 2 * dim, dim), F32)
    place = pl.BlockSpec((seqs // 2, 1, 2 * dim, dim), lambda h: (0, h, 0, 0))
    return pl.pallas_call(
        local_maps_kernel,
        grid=(heads,),
        in_specs=[
            constant(*x.shape), column, column, constant(*wd.shape), constant(*ws.shape),
            constant(1, heads), constant(1, heads), constant(*mult.shape), constant(*spikes.shape),
        ],
        out_specs=[place, place],
        out_shape=[result, result],
        scratch_shapes=[
            pltpu.VMEM((count, 128), F32),
            pltpu.VMEM((count, 128), F32),
            pltpu.VMEM((count // CHUNK, 128, 128), F32),
        ],
        name="local_maps",
    )(x, wk, wv, wd, ws, speeds.reshape(1, -1), ceilings.reshape(1, -1), mult, spikes)


def new_token_kernel(
    x_ref, wk_ref, wv_ref, wq_ref, wd_ref, ws_ref, speed_ref, ceil_ref, out_ref
):
    head = pl.program_id(0)
    dim = wk_ref.shape[1]
    x = x_ref[...]
    lane = lax.axis_index("tp") * speed_ref.shape[0] + head

    def project(w_ref):
        return dot(x, w_ref[...]).astype(BF16).astype(F32)

    query = unit(silu(project(wq_ref))) * dim ** (-0.5)
    keys = unit(silu(project(wk_ref)))
    values = silu(project(wv_ref))
    decay_pre = pick_lane(dot(x, wd_ref[...]), lane)
    strength_pre = pick_lane(dot(x, ws_ref[...]), lane)
    fading = jnp.exp(-speed_ref[head] * softplus(decay_pre))
    match = jnp.sum(query * keys, axis=-1, keepdims=True) * (
        ceil_ref[head] * jax.nn.sigmoid(strength_pre)
    )
    items = [query, keys, values, jnp.broadcast_to(fading, query.shape), jnp.broadcast_to(match, query.shape)]
    for s in range(x.shape[0]):
        for i, item in enumerate(items):
            out_ref[s, 0, i : i + 1, :] = item[s : s + 1]


def new_token(x, wk, wv, wq, wd, ws, speeds, ceilings, dim):
    seqs, width = x.shape
    heads = speeds.shape[0]
    constant = lambda *shape: pl.BlockSpec(shape, lambda h: (0,) * len(shape))
    column = pl.BlockSpec((width, dim), lambda h: (0, h))
    return pl.pallas_call(
        new_token_kernel,
        grid=(heads,),
        in_specs=[
            constant(*x.shape), column, column, column, constant(*wd.shape), constant(*ws.shape),
            SCALARS, SCALARS,
        ],
        out_specs=pl.BlockSpec((seqs, 1, PAD, dim), lambda h: (0, h, 0, 0)),
        out_shape=jax.ShapeDtypeStruct((seqs, heads, PAD, dim), F32),
        name="new_token",
    )(x, wk, wv, wq, wd, ws, speeds, ceilings)


def joined(keep, got, bit, dim):
    early = jnp.where(bit == 0, keep, got)
    late = jnp.where(bit == 0, got, keep)
    early = jnp.concatenate([early[:dim], early[dim:]], axis=1)
    both = dot3(late[:dim], early)
    return both[:, :dim], both[:, dim:] + late[dim:]


def join_kernel(keep_ref, got_ref, *outs, stage, split):
    states, rows, dim = keep_ref.shape
    place = lax.axis_index("sp")
    bit = (place >> stage) % 2
    half = states // 2 if split else states
    following = (place >> (stage + 1)) % 2
    for which, out in enumerate(outs):
        for i in range(half):
            at = i + half * (following ^ which) if split else i
            out_a, out_b = joined(keep_ref[at], got_ref[at], bit, dim)
            out[i, :dim, :] = out_a
            out[i, dim:, :] = out_b


def join(keep, got, stage, split):
    states, rows, dim = keep.shape
    count = states // 2 if split else states
    shape = jax.ShapeDtypeStruct((count, rows, dim), F32)
    return pl.pallas_call(
        lambda *refs: join_kernel(*refs, stage=stage, split=split),
        in_specs=[WHOLE, WHOLE],
        out_specs=[WHOLE] * (2 if split else 1),
        out_shape=[shape] * (2 if split else 1),
        name="join",
    )(keep, got)


def state_of(index, place, seqs, heads, split_bits):
    states = seqs * heads
    base = 0
    for b in range(split_bits):
        states //= 2
        base = base + ((place >> b) % 2) * states
    at = base + index
    return at // heads, at % heads


def pack_kernel(keep_ref, got_ref, token_ref, own_ref, send_ref, *, stage, split_bits):
    states, rows, dim = keep_ref.shape
    seqs, heads = token_ref.shape[:2]
    place = lax.axis_index("sp")
    bit = (place >> stage) % 2
    right = (place >> (stage + 1)) % 2 == 1
    half = dim // 2
    for i in range(states):
        s, h = state_of(i, place, seqs, heads, split_bits)
        out_a, out_b = joined(keep_ref[i], got_ref[i], bit, dim)
        token = token_ref[s, h][:2]
        reads = dot3(jnp.concatenate([token, token, token, token], axis=0), jnp.concatenate([out_a, out_b], axis=1))
        tail = jnp.concatenate([reads[:2, :dim], reads[:2, dim:], reads[:4, :dim]], axis=0)
        own_ref[i, :half, :] = jnp.where(right, out_a[half:], out_b[:half])
        own_ref[i, half:dim, :] = jnp.where(right, out_b[half:], out_b[half:])
        own_ref[i, dim:, :] = tail
        send_ref[i, :half, :] = jnp.where(right, out_a[:half], out_b[:half])
        send_ref[i, half:dim, :] = jnp.where(right, out_b[:half], out_b[half:])
        send_ref[i, dim:, :] = tail


def pack(keep, got, token, stage, split_bits):
    states, rows, dim = keep.shape
    shape = jax.ShapeDtypeStruct((states, dim + PAD, dim), F32)
    return pl.pallas_call(
        lambda *refs: pack_kernel(*refs, stage=stage, split_bits=split_bits),
        in_specs=[WHOLE] * 3,
        out_specs=[WHOLE] * 2,
        out_shape=[shape] * 2,
        name="pack",
    )(keep, got, token)


def finish_kernel(own_ref, got_ref, token_ref, gain_ref, *rest, stage, split_bits, block):
    outs, rows_s = rest[:-1], rest[-1]
    states, _, dim = own_ref.shape
    seqs, heads = token_ref.shape[:2]
    place = lax.axis_index("sp")
    right = (place >> stage) % 2 == 1
    half = dim // 2
    reads = []
    for i in range(states):
        s, h = state_of(i, place, seqs, heads, split_bits)
        own, got = own_ref[i], got_ref[i]
        state = jnp.where(right, got[:dim], own[:dim])
        later = jnp.where(right, own, got)
        full = dot3(jnp.concatenate([later[:half], later[dim:]], axis=0), state)
        rows_s[i] = full[:half] + later[half:dim]
        seen = full[half : half + 2] + later[dim + 2 : dim + 4]
        token = token_ref[s, h]
        fading, match = token[3:4], token[4:5]
        mixed = fading * (seen[:1] - match * seen[1:2]) + match * token[2:3]
        scale = lax.rsqrt(jnp.mean(mixed * mixed, axis=-1, keepdims=True) + EPS)
        reads.append(mixed * scale * gain_ref[...])
    blocks = half // block
    for mask, out in enumerate(outs):
        start = ((place ^ mask) % blocks) * block
        for i in range(states):
            out[i * block : (i + 1) * block, :] = rows_s[i, pl.ds(start, block), :]
            out[states * block + i : states * block + i + 1, :] = reads[i]


def finish(own, got, token, gain, stage, split_bits, block):
    states, _, dim = own.shape
    rows = -(-(states * block + states) // PAD) * PAD
    shape = jax.ShapeDtypeStruct((rows, dim), F32)
    count = 2**split_bits
    return pl.pallas_call(
        lambda *refs: finish_kernel(
            *refs, stage=stage, split_bits=split_bits, block=block
        ),
        in_specs=[WHOLE] * 4,
        out_specs=[WHOLE] * count,
        out_shape=[shape] * count,
        scratch_shapes=[pltpu.VMEM((states, dim // 2, dim), F32)],
        name="finish",
    )(own, got, token, gain.reshape(1, -1))


def place_kernel(*refs, count, split_bits, block):
    ins, cache_ref, read_ref, reads_s = refs[:count], refs[count], refs[count + 1], refs[count + 2]
    seqs, heads, _, dim = cache_ref.shape
    states = seqs * heads // count
    place = lax.axis_index("sp")
    for mask, got in enumerate(ins):
        for i in range(states):
            s, h = state_of(i, place ^ mask, seqs, heads, split_bits)
            cache_ref[s, h] = got[i * block : (i + 1) * block, :].astype(BF16)
            reads_s[pl.ds(s * heads + h, 1), :] = got[states * block + i : states * block + i + 1, :]
    for h in range(heads):
        rows = [reads_s[s * heads + h : s * heads + h + 1, :] for s in range(seqs)]
        read_ref[:, h * dim : (h + 1) * dim] = jnp.concatenate(rows, axis=0).astype(BF16)


def place_outputs(parts, seqs, heads, dim, block, split_bits):
    count = len(parts)
    return pl.pallas_call(
        lambda *refs: place_kernel(*refs, count=count, split_bits=split_bits, block=block),
        in_specs=[WHOLE] * count,
        out_specs=[WHOLE] * 2,
        out_shape=[
            jax.ShapeDtypeStruct((seqs, heads, block, dim), BF16),
            jax.ShapeDtypeStruct((seqs, heads * dim), BF16),
        ],
        scratch_shapes=[pltpu.VMEM((seqs * heads, dim), F32)],
        name="place_outputs",
    )(*parts)


def on_device(
    prompt_elements, address_weights, content_weights, lookup_weights, forgetting_weights,
    update_intensity_weights, forgetting_speeds, update_intensity_ceiling, forgetting_multiplier,
    spike_offsets, upcoming_element_vector, retrieval_rms_multiplier,
):
    seqs = prompt_elements.shape[0]
    dim = retrieval_rms_multiplier.shape[0]
    heads = forgetting_speeds.shape[0]
    places = lax.axis_size("sp")
    stages = places.bit_length() - 1
    block = dim // places

    def exchange(values, mask):
        return lax.ppermute(values, "sp", [(i, i ^ mask) for i in range(places)])

    keep, send = local_maps(
        prompt_elements, address_weights, content_weights, forgetting_weights,
        update_intensity_weights, forgetting_speeds, update_intensity_ceiling,
        forgetting_multiplier, spike_offsets, dim,
    )
    states = seqs * heads // 2
    keep = keep.reshape(states, 2 * dim, dim)
    got = exchange(send.reshape(states, 2 * dim, dim), 1)
    token = new_token(
        upcoming_element_vector, address_weights, content_weights, lookup_weights,
        forgetting_weights, update_intensity_weights, forgetting_speeds,
        update_intensity_ceiling, dim,
    )
    split_bits = 1
    for stage in range(stages - 2):
        split = states % 2 == 0 and split_bits == stage + 1
        if split:
            keep, send = join(keep, got, stage, True)
            states //= 2
            split_bits += 1
        else:
            (keep,) = join(keep, got, stage, False)
            send = keep
        got = exchange(send, 2 ** (stage + 1))
    own, send = pack(keep, got, token, stages - 2, split_bits)
    got = exchange(send, 2 ** (stages - 1))
    parts = finish(own, got, token, retrieval_rms_multiplier, stages - 1, split_bits, block)
    parts = [part if mask == 0 else exchange(part, mask) for mask, part in enumerate(parts)]
    cache, read = place_outputs(parts, seqs, heads, dim, block, split_bits)
    return cache, read


def solution(mesh):
    in_specs = (
        P("gr", "sp", None),
        P(None, "tp"),
        P(None, "tp"),
        P(None, "tp"),
        P(),
        P(),
        P("tp"),
        P("tp"),
        P("gr", "sp", "tp"),
        P("gr", "sp", "tp"),
        P("gr", None),
        P(),
    )
    out_specs = (P("gr", "tp", "sp", None), P("gr", "tp"))
    return jax.shard_map(
        on_device, mesh=mesh, in_specs=in_specs, out_specs=out_specs, check_vma=False
    )
```

profile of v0, /device:TPU:0, one launch (start us, length us, event | category | flops | bytes accessed | tf_op | source)
XLA Modules:
  0.0 95.0 jit_solution(431276375427040404)
XLA Ops:
  0.6 1.8 %copy.14.wd_ref = bf16[2048,8]{1,0:T(8,128)(2,1)} copy(bf16[2048,8]{0,1:T(8,128)(2,1)} %param.16) | data formatting | bytes 65536 | tf_op args[4]
  2.4 1.8 %copy.15.ws_ref = bf16[2048,8]{1,0:T(8,128)(2,1)} copy(bf16[2048,8]{0,1:T(8,128)(2,1)} %param.17) | data formatting | bytes 65536 | tf_op args[5]
  4.2 1.5 %copy.16.mult_ref = f32[2,256,4]{2,1,0:T(8,128)} copy(f32[2,256,4]{1,2,0:T(4,128)} %param.20) | data formatting | bytes 16384 | tf_op args[8]
  5.7 1.5 %copy.17.spike_ref = f32[2,256,4]{2,1,0:T(8,128)} copy(f32[2,256,4]{1,2,0:T(4,128)} %param.21) | data formatting | bytes 16384 | tf_op args[9]
  7.3 39.0 %local_maps.1 = (f32[1,4,256,128]{3,2,1,0:T(8,128)}, f32[1,4,256,128]{3,2,1,0:T(8,128)}) custom-call(bf16[2,256,2048]{2,1,0:T(8,128)(2,1)} %x_ref.2, bf16[2048,512]{1,0:T(8,128)(2,1)} %wk_ref.3, bf16[2048,512]{1,0:T(8,128)(2,1)} %wv_ref.3, bf16[2048,8]{1,0:T(8,128)(2,1)} %copy.14.wd_ref, bf16[2048,8]{1,0:T(8,128)(2,1)} %copy.15.ws_ref, f32[1,4]{1,0:T(1,128)} %bitcast.6, ...), custom_call_target="tpu_custom_call" | custom-call | tf_op jit(solution)/shard_map/local_maps/pallas_call | solution.py:181
  46.3 3.0 %collective-permute-start = (f32[4,256,128]{2,1,0:T(8,128)}, f32[4,256,128]{2,1,0:T(8,128)S(1)}, u32[]{:S(2)}, u32[]{:S(2)}) collective-permute-start(f32[4,256,128]{2,1,0:T(8,128)} %bitcast.9), channel_id=1, source_target_pairs={{0,2},{2,0},{4,6},{6,4},{8,10},{10,8},{12,14},{14,12},{1,3},{3,1},... | collective-permute-start | bytes 1572872 | tf_op jit(solution)/shard_map/ppermute | solution.py:410
  49.3 12.1 %collective-permute-done.refs_1_ = f32[4,256,128]{2,1,0:T(8,128)S(1)} collective-permute-done((f32[4,256,128]{2,1,0:T(8,128)}, f32[4,256,128]{2,1,0:T(8,128)S(1)}, u32[]{:S(2)}, u32[]{:S(2)}) %collective-permute-start) | collective-permute-done | bytes 524320 | tf_op jit(solution)/shard_map/ppermute | solution.py:410
  61.4 0.8 copy-done
  62.2 2.3 %join.1 = (f32[2,256,128]{2,1,0:T(8,128)}, f32[2,256,128]{2,1,0:T(8,128)}) custom-call(f32[4,256,128]{2,1,0:T(8,128)} %bitcast.5, f32[4,256,128]{2,1,0:T(8,128)} %copy-done), custom_call_target="tpu_custom_call" | custom-call | tf_op jit(solution)/shard_map/join/pallas_call | solution.py:269
  64.5 1.8 %collective-permute-start.1 = (f32[2,256,128]{2,1,0:T(8,128)}, f32[2,256,128]{2,1,0:T(8,128)S(1)}, u32[]{:S(2)}, u32[]{:S(2)}) collective-permute-start(f32[2,256,128]{2,1,0:T(8,128)} %get-tuple-element.15), channel_id=1, source_target_pairs={{0,4},{2,6},{4,0},{6,2},{8,12},{10,14},{12,8},{14,10},{1,5},{3,7},... | collective-permute-start | bytes 786440 | tf_op jit(solution)/shard_map/ppermute | solution.py:410
  66.3 5.7 %new_token.1.refs_2_ = f32[2,4,8,128]{3,2,1,0:T(8,128)} custom-call(bf16[2,2048]{1,0:T(2,128)(2,1)} %x_ref.3, bf16[2048,512]{1,0:T(8,128)(2,1)} %wk_ref.3, bf16[2048,512]{1,0:T(8,128)(2,1)} %wv_ref.3, bf16[2048,512]{1,0:T(8,128)(2,1)} %wq_ref.1, bf16[2048,8]{1,0:T(8,128)(2,1)} %copy.14.wd_ref, bf16[2048,8]{1,0:T(8,128)(2,1)} %copy.15.ws_ref, f32[4]{0:T(128)} %speed_ref.1, ...), custom_call_target="tpu_custom_call" | custom-call | tf_op jit(solution)/shard_map/new_token/pallas_call | solution.py:230
  72.2 0.7 copy-done.1
  72.9 2.4 %pack.1 = (f32[2,136,128]{2,1,0:T(8,128)}, f32[2,136,128]{2,1,0:T(8,128)}) custom-call(f32[2,256,128]{2,1,0:T(8,128)} %get-tuple-element.14.refs_0_, f32[2,256,128]{2,1,0:T(8,128)} %copy-done.1, f32[2,4,8,128]{3,2,1,0:T(8,128)} %new_token.1.refs_2_), custom_call_target="tpu_custom_call" | custom-call | tf_op jit(solution)/shard_map/pack/pallas_call | solution.py:312
  75.3 2.5 %collective-permute-start.2 = (f32[2,136,128]{2,1,0:T(8,128)}, f32[2,136,128]{2,1,0:T(8,128)S(1)}, u32[]{:S(2)}, u32[]{:S(2)}) collective-permute-start(f32[2,136,128]{2,1,0:T(8,128)} %get-tuple-element.17), channel_id=1, source_target_pairs={{0,8},{2,10},{4,12},{6,14},{8,0},{10,2},{12,4},{14,6},{1,9},{3,11}... | collective-permute-start | bytes 417800 | tf_op jit(solution)/shard_map/ppermute | solution.py:410
  77.8 5.7 %collective-permute-done.2.refs_1_ = f32[2,136,128]{2,1,0:T(8,128)S(1)} collective-permute-done((f32[2,136,128]{2,1,0:T(8,128)}, f32[2,136,128]{2,1,0:T(8,128)S(1)}, u32[]{:S(2)}, u32[]{:S(2)}) %collective-permute-start.2) | collective-permute-done | bytes 139296 | tf_op jit(solution)/shard_map/ppermute | solution.py:410
  83.5 0.7 copy-done.2
  84.2 1.9 %finish.1 = (f32[40,128]{1,0:T(8,128)}, f32[40,128]{1,0:T(8,128)}, f32[40,128]{1,0:T(8,128)}, f32[40,128]{1,0:T(8,128)}) custom-call(f32[2,136,128]{2,1,0:T(8,128)} %get-tuple-element.16.refs_0_, f32[2,136,128]{2,1,0:T(8,128)} %copy-done.2, f32[2,4,8,128]{3,2,1,0:T(8,128)} %new_token.1.refs_2_, f32[1,128]{1,0:T(1,128)} %bitcast.8), custom_call_target="tpu_custom_call" | custom-call | tf_op jit(solution)/shard_map/finish/pallas_call | solution.py:355
  86.1 1.5 %collective-permute-start.3 = (f32[40,128]{1,0:T(8,128)}, f32[40,128]{1,0:T(8,128)S(1)}, u32[]{:S(2)}, u32[]{:S(2)}) collective-permute-start(f32[40,128]{1,0:T(8,128)} %get-tuple-element.19), channel_id=1, source_target_pairs={{0,2},{2,0},{4,6},{6,4},{8,10},{10,8},{12,14},{14,12},{1,3},{3,1},... | collective-permute-start | bytes 61448 | tf_op jit(solution)/shard_map/ppermute | solution.py:410
  88.0 1.5 %collective-permute-start.5 = (f32[40,128]{1,0:T(8,128)}, f32[40,128]{1,0:T(8,128)S(1)}, u32[]{:S(2)}, u32[]{:S(2)}) collective-permute-start(f32[40,128]{1,0:T(8,128)} %get-tuple-element.21), channel_id=1, source_target_pairs={{0,6},{2,4},{4,2},{6,0},{8,14},{10,12},{12,10},{14,8},{1,7},{3,5},... | collective-permute-start | bytes 61448 | tf_op jit(solution)/shard_map/ppermute | solution.py:410
  89.6 0.5 collective-permute-done.3.refs_1_
  90.1 1.5 %collective-permute-done.4.refs_2_ = f32[40,128]{1,0:T(8,128)S(1)} collective-permute-done((f32[40,128]{1,0:T(8,128)}, f32[40,128]{1,0:T(8,128)S(1)}, u32[]{:S(2)}, u32[]{:S(2)}) %collective-permute-start.4) | collective-permute-done | bytes 20512 | tf_op jit(solution)/shard_map/ppermute | solution.py:410
  91.6 1.3 %collective-permute-done.5.refs_3_ = f32[40,128]{1,0:T(8,128)S(1)} collective-permute-done((f32[40,128]{1,0:T(8,128)}, f32[40,128]{1,0:T(8,128)S(1)}, u32[]{:S(2)}, u32[]{:S(2)}) %collective-permute-start.5) | collective-permute-done | bytes 20512 | tf_op jit(solution)/shard_map/ppermute | solution.py:410
  92.9 0.6 copy-done.5
  93.5 1.4 %place_outputs.1 = (bf16[2,4,16,128]{3,2,1,0:T(8,128)(2,1)}, bf16[2,512]{1,0:T(2,128)(2,1)}) custom-call(f32[40,128]{1,0:T(8,128)} %get-tuple-element.18.refs_0_, f32[40,128]{1,0:T(8,128)} %copy-done.3, f32[40,128]{1,0:T(8,128)} %copy-done.4, f32[40,128]{1,0:T(8,128)} %copy-done.5), custom_call_target="tpu_custom_call" | custom-call | tf_op jit(solution)/shard_map/place_outputs/pallas_call | solution.py:384
  (10 shorter events, 0.6 us)
Async XLA Ops:
  46.3 15.1 %collective-permute-start = (f32[4,256,128]{2,1,0:T(8,128)}, f32[4,256,128]{2,1,0:T(8,128)S(1)}, u32[]{:S(2)}, u32[]{:S(2)}) collective-permute-start(f32[4,256,128]{2,1,0:T(8,128)} %bitcast.9), channel_id=1, source_target_pairs={{0,2},{2,0},{4,6},{6,4},{8,10},{10,8},{12,14},{14,12},{1,3},{3,1},... | collective-permute-start | bytes 1572872 | tf_op jit(solution)/shard_map/ppermute | solution.py:410
  61.4 0.8 copy-start
  64.5 7.7 %collective-permute-start.1 = (f32[2,256,128]{2,1,0:T(8,128)}, f32[2,256,128]{2,1,0:T(8,128)S(1)}, u32[]{:S(2)}, u32[]{:S(2)}) collective-permute-start(f32[2,256,128]{2,1,0:T(8,128)} %get-tuple-element.15), channel_id=1, source_target_pairs={{0,4},{2,6},{4,0},{6,2},{8,12},{10,14},{12,8},{14,10},{1,5},{3,7},... | collective-permute-start | bytes 786440 | tf_op jit(solution)/shard_map/ppermute | solution.py:410
  72.2 0.7 copy-start.1
  75.3 8.2 %collective-permute-start.2 = (f32[2,136,128]{2,1,0:T(8,128)}, f32[2,136,128]{2,1,0:T(8,128)S(1)}, u32[]{:S(2)}, u32[]{:S(2)}) collective-permute-start(f32[2,136,128]{2,1,0:T(8,128)} %get-tuple-element.17), channel_id=1, source_target_pairs={{0,8},{2,10},{4,12},{6,14},{8,0},{10,2},{12,4},{14,6},{1,9},{3,11}... | collective-permute-start | bytes 417800 | tf_op jit(solution)/shard_map/ppermute | solution.py:410
  83.5 0.7 copy-start.2
  86.1 4.0 %collective-permute-start.3 = (f32[40,128]{1,0:T(8,128)}, f32[40,128]{1,0:T(8,128)S(1)}, u32[]{:S(2)}, u32[]{:S(2)}) collective-permute-start(f32[40,128]{1,0:T(8,128)} %get-tuple-element.19), channel_id=1, source_target_pairs={{0,2},{2,0},{4,6},{6,4},{8,10},{10,8},{12,14},{14,12},{1,3},{3,1},... | collective-permute-start | bytes 61448 | tf_op jit(solution)/shard_map/ppermute | solution.py:410
  87.6 4.0 %collective-permute-start.4 = (f32[40,128]{1,0:T(8,128)}, f32[40,128]{1,0:T(8,128)S(1)}, u32[]{:S(2)}, u32[]{:S(2)}) collective-permute-start(f32[40,128]{1,0:T(8,128)} %get-tuple-element.20), channel_id=1, source_target_pairs={{0,4},{2,6},{4,0},{6,2},{8,12},{10,14},{12,8},{14,10},{1,5},{3,7},... | collective-permute-start | bytes 61448 | tf_op jit(solution)/shard_map/ppermute | solution.py:410
  88.0 4.9 %collective-permute-start.5 = (f32[40,128]{1,0:T(8,128)}, f32[40,128]{1,0:T(8,128)S(1)}, u32[]{:S(2)}, u32[]{:S(2)}) collective-permute-start(f32[40,128]{1,0:T(8,128)} %get-tuple-element.21), channel_id=1, source_target_pairs={{0,6},{2,4},{4,2},{6,0},{8,14},{10,12},{12,10},{14,8},{1,7},{3,5},... | collective-permute-start | bytes 61448 | tf_op jit(solution)/shard_map/ppermute | solution.py:410
  90.1 2.9 %copy-start.3 = (f32[40,128]{1,0:T(8,128)}, f32[40,128]{1,0:T(8,128)S(1)}, u32[]{:S(2)}) copy-start(f32[40,128]{1,0:T(8,128)S(1)} %collective-permute-done.3.refs_1_) | copy-start | bytes 61444
  91.6 1.3 %copy-start.4 = (f32[40,128]{1,0:T(8,128)}, f32[40,128]{1,0:T(8,128)S(1)}, u32[]{:S(2)}) copy-start(f32[40,128]{1,0:T(8,128)S(1)} %collective-permute-done.4.refs_2_) | copy-start | bytes 61444
  92.9 0.6 copy-start.5
where the time goes:
time: 95.5 us; the launch traced here: 95 us
  Pallas kernels  52.8 us (55%)
  waiting for transfers between devices  21.3 us (22%)
  starting transfers between devices  10.8 us (11%)
  local copies, waits for them, and re-layouts  9.4 us (10%)
    pallas_call x1, Pallas kernels, local_maps(): pl.pallas_call(local_maps_kernel, grid=(heads,), in_specs=[constant(*x.sh...  39 us
    ppermute x6, waiting for transfers between devices, exchange(): return lax.ppermute(values, 'sp', [(i, i ^ mask) for i in range(places)])  21.3 us
    ppermute x6, starting transfers between devices, exchange(): return lax.ppermute(values, 'sp', [(i, i ^ mask) for i in range(places)])  10.8 us
    unnamed x16, local copies, waits for them, and re-layouts  9.4 us
    pallas_call x1, Pallas kernels, new_token(): pl.pallas_call(new_token_kernel, grid=(heads,), in_specs=[constant(*x.sha...  5.71 us
    pallas_call x1, Pallas kernels, pack(): pl.pallas_call(lambda *refs: pack_kernel(*refs, stage=stage, split_bits=s...  2.4 us
    pallas_call x1, Pallas kernels, join(): pl.pallas_call(lambda *refs: join_kernel(*refs, stage=stage, split=split)...  2.3 us
    pallas_call x1, Pallas kernels, finish(): pl.pallas_call(lambda *refs: finish_kernel(*refs, stage=stage, split_bits...  1.93 us
  transfers between devices with their start and end apart: 6, of which 6 were waited for; matrix products, arithmetic and copies ran while one was open for 0% of the time, Pallas kernels for 6%

commit v1 on v0

v1 whole, which is shorter than its diff:
```python
import jax
import jax.numpy as jnp
from jax import lax
from jax.experimental import pallas as pl
from jax.experimental.pallas import tpu as pltpu
from jax.sharding import PartitionSpec as P

EPS = 1e-06
CHUNK = 128
PAD = 8
F32 = jnp.float32
BF16 = jnp.bfloat16
WHOLE = pl.BlockSpec(memory_space=pltpu.VMEM)
LIMIT = pltpu.CompilerParams(vmem_limit_bytes=16 * 2**20)


def dot(a, b):
    return jnp.dot(a, b, preferred_element_type=F32)


def dot_nt(a, b):
    return lax.dot_general(a, b, (((1,), (1,)), ((), ())), preferred_element_type=F32)


def dot_tn(a, b):
    return lax.dot_general(a, b, (((0,), (0,)), ((), ())), preferred_element_type=F32)


def halves(a):
    high = a.astype(BF16)
    return high, (a - high.astype(F32)).astype(BF16)


def dot3(a, b):
    ah, al = halves(a)
    bh, bl = halves(b)
    return dot(ah, bh) + dot(ah, bl) + dot(al, bh)


def silu(values):
    return values * jax.nn.sigmoid(values)


def unit(values):
    return values * lax.rsqrt(jnp.sum(values * values, axis=-1, keepdims=True) + EPS)


def softplus(values):
    return jnp.maximum(values, 0.0) + jnp.log1p(jnp.exp(-jnp.abs(values)))


def pick_lane(values, lane):
    places = lax.broadcasted_iota(jnp.int32, values.shape, 1)
    return jnp.sum(jnp.where(places == lane, values, 0.0), axis=1, keepdims=True)


def gate_tables(x, wd, ws, speeds, ceilings, mult, spike, heads, upper):
    total = wd.shape[0]
    rates = jnp.concatenate([wd.astype(F32), ws.astype(F32)], axis=0)
    both = dot_nt(rates.astype(BF16), x)
    shard = lax.axis_index("tp")
    row = lax.broadcasted_iota(jnp.int32, (heads, heads), 0)
    col = lax.broadcasted_iota(jnp.int32, (heads, heads), 1)

    def mine(full):
        part = full[:heads]
        for t in range(1, total // heads):
            part = jnp.where(shard == t, full[t * heads : (t + 1) * heads], part)
        return part

    def upright(values):
        return jnp.sum(jnp.where(row == col, values[:, :heads], 0.0), axis=1, keepdims=True)

    gates = -upright(speeds) * softplus(mine(both[:total])) * mult + spike
    beta = upright(ceilings) * jax.nn.sigmoid(mine(both[total:]))
    rows = []
    for c in range(x.shape[0] // CHUNK):
        lanes = slice(c * CHUNK, (c + 1) * CHUNK)
        rows.append(beta[:, lanes])
        rows.append(
            jnp.dot(gates[:, lanes], upper, precision=lax.Precision.HIGHEST, preferred_element_type=F32)
        )
    fill = -sum(r.shape[0] for r in rows) % PAD
    if fill:
        rows.append(jnp.zeros((fill, CHUNK), F32))
    return jnp.concatenate(rows, axis=0)


def local_maps_kernel(*refs, heads, own_heads, first):
    if first:
        x_hbm, wk_hbm, wv_hbm = refs[:3]
        small_hbm = refs[3:9]
        keep_ref, send_ref, table_ref = refs[9:12]
        k_s, v_s, lower_s, inverse_s, half_s, mask_s, x_s, w_s = refs[12:20]
        small_s = refs[20:26]
        sems = refs[26]
    else:
        x_s, wk_ref, wv_ref, table_ref = refs[:4]
        keep_ref, send_ref = refs[4:6]
        k_s, v_s, lower_s, inverse_s, half_s, mask_s = refs[6:12]
    seqs, span, width = x_s.shape
    dim = k_s.shape[-1]
    count = seqs * span
    chunks = count // CHUNK
    group = len(own_heads)
    steps = [2**i for i in range(CHUNK.bit_length() - 1)]

    if first:
        copies = [pltpu.make_async_copy(x_hbm.at[s], x_s.at[s], sems.at[s]) for s in range(seqs)]
        for i, (source, target) in enumerate(zip(small_hbm, small_s)):
            copies.append(pltpu.make_async_copy(source, target, sems.at[seqs + i]))
        base = len(copies)
        for g, h in enumerate(own_heads):
            for i, w_hbm in enumerate((wk_hbm, wv_hbm)):
                copies.append(
                    pltpu.make_async_copy(
                        w_hbm.at[:, pl.ds(h * dim, dim)],
                        w_s.at[g, :, pl.ds(i * dim, dim)],
                        sems.at[base + 2 * g + i],
                    )
                )
        for copy in copies:
            copy.start()

    row = lax.broadcasted_iota(jnp.int32, (CHUNK, CHUNK), 0)
    col = lax.broadcasted_iota(jnp.int32, (CHUNK, CHUNK), 1)
    strict = row > col
    eye = jnp.where(row == col, 1.0, 0.0)

    def level(m):
        return (row // (2 * m) == col // (2 * m)) & (row // m != col // m)

    for i, m in enumerate(steps):
        mask_s[i] = jnp.where(level(m), 1.0, 0.0).astype(BF16)
    mask_s[len(steps)] = jnp.where(strict, 1.0, 0.0).astype(BF16)

    if first:
        for copy in copies[:base]:
            copy.wait()
    flat = x_s[...].reshape(count, width)
    if first:
        wd, ws, speeds, ceilings = (ref[...] for ref in small_s[:4])
        mult, spike = (
            jnp.concatenate([ref[s] for s in range(seqs)], axis=1) for ref in small_s[4:]
        )
        table_ref[...] = gate_tables(
            flat, wd, ws, speeds, ceilings, mult, spike, heads, jnp.where(row <= col, 1.0, 0.0)
        )
    columns = table_ref[...].T

    def at(c, g, which):
        return (2 * c + which) * heads + own_heads[g]

    def column(c, g, which):
        return jnp.broadcast_to(columns[:, at(c, g, which) : at(c, g, which) + 1], (CHUNK, CHUNK))

    pieces = [(g, c) for g in range(group) for c in range(chunks)]

    for g, h in enumerate(own_heads):
        if first:
            copies[base + 2 * g].wait()
            copies[base + 2 * g + 1].wait()
            weights = w_s[g]
        else:
            lanes = slice(h * dim, (h + 1) * dim)
            weights = jnp.concatenate([wk_ref[:, lanes], wv_ref[:, lanes]], axis=1)
        raw = dot(flat, weights).astype(BF16).astype(F32)
        k_s[g] = unit(silu(raw[:, :dim]))
        v_s[g] = silu(raw[:, dim:])

    def rows_of(c):
        return slice(c * CHUNK, (c + 1) * CHUNK)

    for n, (g, c) in enumerate(pieces):
        short = k_s[g, rows_of(c)].astype(BF16)
        gram = dot_nt(short, short)
        place = at(c, g, 1)
        spread = jnp.exp(jnp.minimum(column(c, g, 1) - table_ref[place : place + 1, :], 0.0))
        lower = jnp.where(strict, gram * column(c, g, 0) * spread, 0.0)
        lower_s[n] = lower.astype(BF16)
        inverse_s[n] = (eye - jnp.where(level(1), lower, 0.0)).astype(BF16)

    for i, m in list(enumerate(steps))[1:]:
        odd = [slice(o, o + m) for o in range(m, CHUNK, 2 * m)]
        if m < 16:
            for n in range(len(pieces)):
                half_s[n] = dot(inverse_s[n], lower_s[n] * mask_s[i]).astype(BF16)
            for n in range(len(pieces)):
                inverse_s[n] = inverse_s[n] - dot(half_s[n], inverse_s[n]).astype(BF16)
        else:
            for n in range(len(pieces)):
                picked = jnp.concatenate([inverse_s[n, o] for o in odd], axis=0)
                half_s[n, : CHUNK // 2] = dot(picked, lower_s[n] * mask_s[i]).astype(BF16)
            for n in range(len(pieces)):
                change = dot(half_s[n, : CHUNK // 2], inverse_s[n]).astype(BF16)
                for j, o in enumerate(odd):
                    inverse_s[n, o] = inverse_s[n, o] - change[j * m : (j + 1) * m]

    terms = []
    for n, (g, c) in enumerate(pieces):
        keys, values = k_s[g, rows_of(c)], v_s[g, rows_of(c)]
        strength, total_log = column(c, g, 0), column(c, g, 1)
        last = total_log[CHUNK - 1 : CHUNK]
        off = inverse_s[n] * mask_s[len(steps)]
        source = jnp.concatenate([keys * (strength * jnp.exp(total_log)), values * strength], axis=1)
        solved = source + dot(off, source.astype(BF16))
        faded = (keys * jnp.exp(last - total_log)).astype(BF16)
        change = dot_tn(faded, solved.astype(BF16))
        terms.append((change[:, :dim], change[:, dim:], jnp.exp(last)))

    bit = lax.axis_index("sp") % 2
    half = seqs // 2
    per = chunks // seqs
    for g in range(group):
        maps = []
        for s in range(seqs):
            mine = terms[g * chunks + s * per : g * chunks + (s + 1) * per]
            eraser, target, decay = mine[0]
            held_a, held_b = decay * eye - eraser, target
            for eraser, target, decay in mine[1:]:
                change = dot(
                    eraser.astype(BF16), jnp.concatenate([held_a, held_b], axis=1).astype(BF16)
                )
                held_a = decay * held_a - change[:, :dim]
                held_b = decay * held_b - change[:, dim:] + target
            maps.append((held_a, held_b))
        for s in range(half):
            for part in range(2):
                one, two = maps[s][part], maps[s + half][part]
                rows = slice(part * dim, (part + 1) * dim)
                keep_ref[s * group + g, rows, :] = jnp.where(bit == 0, one, two)
                send_ref[s * group + g, rows, :] = jnp.where(bit == 0, two, one)


def local_maps(x, wk, wv, small, heads, own_heads, dim, table=None):
    seqs, span, width = x.shape
    count = seqs * span
    group = len(own_heads)
    pieces = group * count // CHUNK
    square = (CHUNK, CHUNK)
    result = pltpu.VMEM((seqs // 2 * group, 2 * dim, dim), F32)
    scratch = [
        pltpu.VMEM((group, count, dim), F32),
        pltpu.VMEM((group, count, dim), F32),
        pltpu.VMEM((pieces,) + square, BF16),
        pltpu.VMEM((pieces,) + square, BF16),
        pltpu.VMEM((pieces,) + square, BF16),
        pltpu.VMEM((CHUNK.bit_length(),) + square, BF16),
    ]
    first = table is None
    if first:
        rows = -(-2 * heads * (count // CHUNK) // PAD) * PAD
        scratch += [pltpu.VMEM(x.shape, BF16), pltpu.VMEM((group, width, 2 * dim), BF16)]
        scratch += [pltpu.VMEM(a.shape, a.dtype) for a in small]
        scratch.append(pltpu.SemaphoreType.DMA((seqs + len(small) + 2 * group,)))
        operands = [pltpu.with_memory_space_constraint(a, pltpu.HBM) for a in (x, wk, wv, *small)]
        in_specs = [pl.BlockSpec(memory_space=pltpu.HBM)] * len(operands)
        results = [result, result, pltpu.VMEM((rows, CHUNK), F32)]
    else:
        operands = [x, wk, wv, table]
        in_specs = [WHOLE] * 4
        results = [result, result]
    return pl.pallas_call(
        lambda *refs: local_maps_kernel(*refs, heads=heads, own_heads=own_heads, first=first),
        in_specs=in_specs,
        out_specs=[WHOLE] * len(results),
        out_shape=results,
        scratch_shapes=scratch,
        compiler_params=pltpu.CompilerParams(vmem_limit_bytes=24 * 2**20),
        name="local_maps",
    )(*operands)


def new_token_kernel(
    x_ref, wk_ref, wv_ref, wq_ref, wd_ref, ws_ref, speed_ref, ceil_ref, out_ref
):
    head = pl.program_id(0)
    dim = wk_ref.shape[1]
    x = x_ref[...]
    lane = lax.axis_index("tp") * speed_ref.shape[1] + head

    def project(w_ref):
        return dot(x, w_ref[...]).astype(BF16).astype(F32)

    query = unit(silu(project(wq_ref))) * dim ** (-0.5)
    keys = unit(silu(project(wk_ref)))
    values = silu(project(wv_ref))
    decay_pre = pick_lane(dot_nt(x, wd_ref[...]), lane)
    strength_pre = pick_lane(dot_nt(x, ws_ref[...]), lane)
    fading = jnp.exp(-pick_lane(speed_ref[...], head) * softplus(decay_pre))
    match = jnp.sum(query * keys, axis=-1, keepdims=True) * (
        pick_lane(ceil_ref[...], head) * jax.nn.sigmoid(strength_pre)
    )
    items = [query, keys, values, jnp.broadcast_to(fading, query.shape), jnp.broadcast_to(match, query.shape)]
    for s in range(x.shape[0]):
        for i, item in enumerate(items):
            out_ref[s, 0, i : i + 1, :] = item[s : s + 1]


def new_token(x, wk, wv, wq, wd, ws, speeds, ceilings, dim):
    seqs, width = x.shape
    heads = speeds.shape[0]
    constant = lambda *shape: pl.BlockSpec(shape, lambda h: (0,) * len(shape))
    column = pl.BlockSpec((width, dim), lambda h: (0, h))
    return pl.pallas_call(
        new_token_kernel,
        grid=(heads,),
        in_specs=[
            constant(*x.shape), column, column, column, constant(wd.shape[1], width),
            constant(ws.shape[1], width), constant(1, heads), constant(1, heads),
        ],
        out_specs=pl.BlockSpec((seqs, 1, PAD, dim), lambda h: (0, h, 0, 0)),
        out_shape=pltpu.VMEM((seqs, heads, PAD, dim), F32),
        compiler_params=LIMIT,
        name="new_token",
    )(x, wk, wv, wq, wd.T, ws.T, speeds.reshape(1, -1), ceilings.reshape(1, -1))


def joined(keep, got, bit, dim):
    early = jnp.where(bit == 0, keep, got)
    late = jnp.where(bit == 0, got, keep)
    early = jnp.concatenate([early[:dim], early[dim:]], axis=1)
    both = dot3(late[:dim], early)
    return both[:, :dim], both[:, dim:] + late[dim:]


def join_kernel(keep_ref, got_ref, *outs, stage, split):
    states, rows, dim = keep_ref.shape
    place = lax.axis_index("sp")
    bit = (place >> stage) % 2
    half = states // 2 if split else states
    following = (place >> (stage + 1)) % 2
    for which, out in enumerate(outs):
        for i in range(half):
            at = i + half * (following ^ which) if split else i
            out_a, out_b = joined(keep_ref[at], got_ref[at], bit, dim)
            out[i, :dim, :] = out_a
            out[i, dim:, :] = out_b


def join(keep, got, stage, split):
    states, rows, dim = keep.shape
    count = states // 2 if split else states
    shape = pltpu.VMEM((count, rows, dim), F32)
    return pl.pallas_call(
        lambda *refs: join_kernel(*refs, stage=stage, split=split),
        in_specs=[WHOLE, WHOLE],
        out_specs=[WHOLE] * (2 if split else 1),
        out_shape=[shape] * (2 if split else 1),
        compiler_params=LIMIT,
        name="join",
    )(keep, got)


def state_of(index, place, seqs, heads, split_bits):
    states = seqs * heads
    base = 0
    for b in range(split_bits):
        states //= 2
        base = base + ((place >> b) % 2) * states
    at = base + index
    return at // heads, at % heads


def pack_kernel(keep_ref, got_ref, token_ref, own_ref, send_ref, *, stage, split_bits, own_heads):
    states, rows, dim = keep_ref.shape
    seqs = token_ref.shape[0]
    place = lax.axis_index("sp")
    bit = (place >> stage) % 2
    right = (place >> (stage + 1)) % 2 == 1
    half = dim // 2
    for i in range(states):
        s, h = state_of(i, place, seqs, len(own_heads), split_bits)
        out_a, out_b = joined(keep_ref[i], got_ref[i], bit, dim)
        token = token_ref[s, h + own_heads[0]][:2]
        reads = dot3(jnp.concatenate([token, token, token, token], axis=0), jnp.concatenate([out_a, out_b], axis=1))
        tail = jnp.concatenate([reads[:2, :dim], reads[:2, dim:], reads[:4, :dim]], axis=0)
        own_ref[i, :half, :] = jnp.where(right, out_a[half:], out_b[:half])
        own_ref[i, half:dim, :] = jnp.where(right, out_b[half:], out_b[half:])
        own_ref[i, dim:, :] = tail
        send_ref[i, :half, :] = jnp.where(right, out_a[:half], out_b[:half])
        send_ref[i, half:dim, :] = jnp.where(right, out_b[:half], out_b[half:])
        send_ref[i, dim:, :] = tail


def pack(keep, got, token, stage, split_bits, own_heads):
    states, rows, dim = keep.shape
    shape = pltpu.VMEM((states, dim + PAD, dim), F32)
    return pl.pallas_call(
        lambda *refs: pack_kernel(
            *refs, stage=stage, split_bits=split_bits, own_heads=own_heads
        ),
        in_specs=[WHOLE] * 3,
        out_specs=[WHOLE] * 2,
        out_shape=[shape] * 2,
        compiler_params=LIMIT,
        name="pack",
    )(keep, got, token)


def finish_kernel(*refs, groups, stage, split_bits, block):
    count = len(groups)
    owns, gots = refs[:count], refs[count : 2 * count]
    token_ref, gain_ref = refs[2 * count : 2 * count + 2]
    outs, rows_s = refs[2 * count + 2 : -1], refs[-1]
    states, _, dim = owns[0].shape
    seqs = token_ref.shape[0]
    place = lax.axis_index("sp")
    right = (place >> stage) % 2 == 1
    half = dim // 2
    reads = []
    for g, own_heads in enumerate(groups):
        for i in range(states):
            s, h = state_of(i, place, seqs, len(own_heads), split_bits)
            own, got = owns[g][i], gots[g][i]
            state = jnp.where(right, got[:dim], own[:dim])
            later = jnp.where(right, own, got)
            full = dot3(jnp.concatenate([later[:half], later[dim:]], axis=0), state)
            rows_s[g * states + i] = full[:half] + later[half:dim]
            seen = full[half : half + 2] + later[dim + 2 : dim + 4]
            token = token_ref[s, h + own_heads[0]]
            fading, match = token[3:4], token[4:5]
            mixed = fading * (seen[:1] - match * seen[1:2]) + match * token[2:3]
            scale = lax.rsqrt(jnp.mean(mixed * mixed, axis=-1, keepdims=True) + EPS)
            reads.append(mixed * scale * gain_ref[...])
    blocks = half // block
    total = count * states
    for mask, out in enumerate(outs):
        start = ((place ^ mask) % blocks) * block
        for i in range(total):
            out[i * block : (i + 1) * block, :] = rows_s[i, pl.ds(start, block), :]
            out[total * block + i : total * block + i + 1, :] = reads[i]


def finish(owns, gots, token, gain, groups, stage, split_bits, block):
    states, _, dim = owns[0].shape
    total = states * len(groups)
    rows = -(-(total * block + total) // PAD) * PAD
    shape = pltpu.VMEM((rows, dim), F32)
    count = 2**split_bits
    return pl.pallas_call(
        lambda *refs: finish_kernel(
            *refs, groups=groups, stage=stage, split_bits=split_bits, block=block
        ),
        in_specs=[WHOLE] * (2 * len(groups) + 2),
        out_specs=[WHOLE] * count,
        out_shape=[shape] * count,
        scratch_shapes=[pltpu.VMEM((total, dim // 2, dim), F32)],
        compiler_params=LIMIT,
        name="finish",
    )(*owns, *gots, token, gain.reshape(1, -1))


def place_kernel(*refs, groups, count, split_bits, block):
    ins, cache_ref, read_ref, reads_s = refs[:count], refs[count], refs[count + 1], refs[count + 2]
    seqs, heads, _, dim = cache_ref.shape
    total = seqs * heads // count
    states = total // len(groups)
    place = lax.axis_index("sp")
    for mask, got in enumerate(ins):
        for g, own_heads in enumerate(groups):
            for i in range(states):
                s, h = state_of(i, place ^ mask, seqs, len(own_heads), split_bits)
                h = h + own_heads[0]
                n = g * states + i
                cache_ref[s, h] = got[n * block : (n + 1) * block, :].astype(BF16)
                reads_s[pl.ds(s * heads + h, 1), :] = got[total * block + n : total * block + n + 1, :]
    for h in range(heads):
        rows = [reads_s[s * heads + h : s * heads + h + 1, :] for s in range(seqs)]
        read_ref[:, h * dim : (h + 1) * dim] = jnp.concatenate(rows, axis=0).astype(BF16)


def place_outputs(parts, groups, seqs, heads, dim, block, split_bits):
    count = len(parts)
    return pl.pallas_call(
        lambda *refs: place_kernel(
            *refs, groups=groups, count=count, split_bits=split_bits, block=block
        ),
        in_specs=[WHOLE] * count,
        out_specs=[WHOLE] * 2,
        out_shape=[
            jax.ShapeDtypeStruct((seqs, heads, block, dim), BF16),
            jax.ShapeDtypeStruct((seqs, heads * dim), BF16),
        ],
        scratch_shapes=[pltpu.VMEM((seqs * heads, dim), F32)],
        compiler_params=LIMIT,
        name="place_outputs",
    )(*parts)


def on_device(
    prompt_elements, address_weights, content_weights, lookup_weights, forgetting_weights,
    update_intensity_weights, forgetting_speeds, update_intensity_ceiling, forgetting_multiplier,
    spike_offsets, upcoming_element_vector, retrieval_rms_multiplier,
):
    seqs = prompt_elements.shape[0]
    dim = retrieval_rms_multiplier.shape[0]
    heads = forgetting_speeds.shape[0]
    places = lax.axis_size("sp")
    stages = places.bit_length() - 1
    block = dim // places

    def exchange(values, mask):
        got = lax.ppermute(values, "sp", [(i, i ^ mask) for i in range(places)])
        return pltpu.with_memory_space_constraint(got, pltpu.VMEM)

    parts = 2 if heads % 2 == 0 else 1
    size = heads // parts
    groups = [list(range(g * size, (g + 1) * size)) for g in range(parts)]

    def flat_row(values):
        return jnp.concatenate([values] * (2 if heads == 1 else 1)).reshape(1, -1)

    small = (
        forgetting_weights.T, update_intensity_weights.T, flat_row(forgetting_speeds),
        flat_row(update_intensity_ceiling), forgetting_multiplier.transpose(0, 2, 1),
        spike_offsets.transpose(0, 2, 1),
    )
    table = None
    flows = []
    for own_heads in groups:
        results = local_maps(
            prompt_elements, address_weights, content_weights, small, heads, own_heads, dim, table
        )
        if table is None:
            table = results[2]
        flows.append([results[0], exchange(results[1], 1)])
    token = new_token(
        upcoming_element_vector, address_weights, content_weights, lookup_weights,
        forgetting_weights, update_intensity_weights, forgetting_speeds,
        update_intensity_ceiling, dim,
    )
    states = seqs * size // 2
    split_bits = 1
    for stage in range(stages - 2):
        split = states % 2 == 0 and split_bits == stage + 1
        for flow in flows:
            joint = join(flow[0], flow[1], stage, split)
            flow[:] = joint[0], exchange(joint[-1], 2 ** (stage + 1))
        if split:
            states //= 2
            split_bits += 1
    for own_heads, flow in zip(groups, flows):
        own, send = pack(flow[0], flow[1], token, stages - 2, split_bits, own_heads)
        flow[:] = own, exchange(send, 2 ** (stages - 1))
    pieces = finish(
        [flow[0] for flow in flows], [flow[1] for flow in flows], token,
        retrieval_rms_multiplier, groups, stages - 1, split_bits, block,
    )
    pieces = [piece if mask == 0 else exchange(piece, mask) for mask, piece in enumerate(pieces)]
    cache, read = place_outputs(pieces, groups, seqs, heads, dim, block, split_bits)
    return cache, read


def solution(mesh):
    in_specs = (
        P("gr", "sp", None),
        P(None, "tp"),
        P(None, "tp"),
        P(None, "tp"),
        P(),
        P(),
        P("tp"),
        P("tp"),
        P("gr", "sp", "tp"),
        P("gr", "sp", "tp"),
        P("gr", None),
        P(),
    )
    out_specs = (P("gr", "tp", "sp", None), P("gr", "tp"))
    return jax.shard_map(
        on_device, mesh=mesh, in_specs=in_specs, out_specs=out_specs, check_vma=False
    )
```

time: 95.5 us -> 45.7 us (0.48)
  Pallas kernels: 52.8 us -> 17.6 us
  local copies, waits for them, and re-layouts: 9.4 us -> 0.05 us
  waiting for transfers between devices: 21.3 us -> 14.1 us
  starting transfers between devices: 10.8 us -> 13 us
    pallas_call x3 -> x4, Pallas kernels: 42.4 us -> 13.2 us  [the longest x2 12.3 us: local_maps(): pl.pallas_call(lambda *refs: local_maps_kernel(*refs, heads=heads, own_he...]
    unnamed x16 -> x20, local copies, waits for them, and re-layouts: 9.4 us -> 0.05 us
    ppermute x6 -> x9, waiting for transfers between devices: 21.3 us -> 14.1 us  [exchange(): got = lax.ppermute(values, 'sp', [(i, i ^ mask) for i in range(places)])]
    pallas_call x1, Pallas kernels: 5.71 us -> 3.07 us  [new_token(): pl.pallas_call(new_token_kernel, grid=(heads,), in_specs=[constant(*x.sha...]
    ppermute x6 -> x9, starting transfers between devices: 10.8 us -> 13 us  [exchange(): got = lax.ppermute(values, 'sp', [(i, i ^ mask) for i in range(places)])]
    pallas_call x1 -> x2, Pallas kernels: 2.3 us -> 0.55 us  [join(): pl.pallas_call(lambda *refs: join_kernel(*refs, stage=stage, split=split)...]
    pallas_call x1 -> x2, Pallas kernels: 2.4 us -> 0.75 us  [pack(): pl.pallas_call(lambda *refs: pack_kernel(*refs, stage=stage, split_bits=s...]
  transfers between devices with their start and end apart: 6 -> 9, of which waited for: 6 -> 7; matrix products, arithmetic and copies ran while one was open for 0% -> 0% of each run, Pallas kernels for 6% -> 19%
where the time goes in v1:
time: 45.7 us; the launch traced here: 45.5 us
  Pallas kernels  17.6 us (39%)
  waiting for transfers between devices  14.1 us (31%)
  starting transfers between devices  13 us (28%)
  between operations  0.79 us (2%)
    ppermute x9, waiting for transfers between devices, exchange(): got = lax.ppermute(values, 'sp', [(i, i ^ mask) for i in range(places)])  14.1 us
    ppermute x9, starting transfers between devices, exchange(): got = lax.ppermute(values, 'sp', [(i, i ^ mask) for i in range(places)])  13 us
    pallas_call x2, Pallas kernels, local_maps(): pl.pallas_call(lambda *refs: local_maps_kernel(*refs, heads=heads, own_he...  12.3 us
    pallas_call x1, Pallas kernels, new_token(): pl.pallas_call(new_token_kernel, grid=(heads,), in_specs=[constant(*x.sha...  3.07 us
  transfers between devices with their start and end apart: 9, of which 7 were waited for; matrix products, arithmetic and copies ran while one was open for 0% of the time, Pallas kernels for 19%

profile of v1, /device:TPU:0, one launch (start us, length us, event | category | flops | bytes accessed | tf_op | source)
XLA Modules:
  0.0 45.5 jit_solution(11103727569293243303)
XLA Ops:
  0.7 8.1 %local_maps.2 = (f32[2,256,128]{2,1,0:T(8,128)S(1)}, f32[2,256,128]{2,1,0:T(8,128)S(1)}, f32[32,128]{1,0:T(8,128)S(1)}) custom-call(bf16[2,256,2048]{2,1,0:T(8,128)(2,1)} %refs_0_.3, bf16[2048,512]{1,0:T(8,128)(2,1)} %refs_1_.3, bf16[2048,512]{1,0:T(8,128)(2,1)} %refs_2_.3, bf16[8,2048]{1,0:T(8,128)(2,1)} %bitcast.7, bf16[8,2048]{1,0:T(8,128)(2,1)} %bitcast.9, ...), custom_call_target="tpu_custom_call" | custom-call | tf_op jit(solution)/shard_map/local_maps/pallas_call | solution.py:263
  8.8 3.1 %collective-permute-start = (f32[2,256,128]{2,1,0:T(8,128)S(1)}, f32[2,256,128]{2,1,0:T(8,128)S(1)}, u32[]{:S(2)}, u32[]{:S(2)}) collective-permute-start(f32[2,256,128]{2,1,0:T(8,128)S(1)} %get-tuple-element.20), channel_id=1, source_target_pairs={{0,2},{2,0},{4,6},{6,4},{8,10},{10,8},{12,14},{14,12},{1,3},{3,1},... | collective-permute-start | bytes 786440 | tf_op jit(solution)/shard_map/ppermute | solution.py:504
  12.0 4.1 %local_maps.3 = (f32[2,256,128]{2,1,0:T(8,128)S(1)}, f32[2,256,128]{2,1,0:T(8,128)S(1)}) custom-call(bf16[2,256,2048]{2,1,0:T(8,128)(2,1)S(1)} %copy-done.2, bf16[2048,512]{1,0:T(8,128)(2,1)S(1)} %copy-done, bf16[2048,512]{1,0:T(8,128)(2,1)S(1)} %copy-done.1, f32[32,128]{1,0:T(8,128)S(1)} %get-tuple-element.24.refs_3_), custom_call_target="tpu_custom_call" | custom-call | tf_op jit(solution)/shard_map/local_maps/pallas_call | solution.py:263
  16.1 0.1 collective-permute-start.2
  16.2 2.4 %collective-permute-done.refs_1_ = f32[2,256,128]{2,1,0:T(8,128)S(1)} collective-permute-done((f32[2,256,128]{2,1,0:T(8,128)S(1)}, f32[2,256,128]{2,1,0:T(8,128)S(1)}, u32[]{:S(2)}, u32[]{:S(2)}) %collective-permute-start) | collective-permute-done | bytes 262176 | tf_op jit(solution)/shard_map/ppermute | solution.py:504
  18.6 0.3 join.2
  18.9 1.6 %collective-permute-start.1 = (f32[1,256,128]{2,1,0:T(8,128)S(1)}, f32[1,256,128]{2,1,0:T(8,128)S(1)}, u32[]{:S(2)}, u32[]{:S(2)}) collective-permute-start(f32[1,256,128]{2,1,0:T(8,128)S(1)} %get-tuple-element.22), channel_id=1, source_target_pairs={{0,4},{2,6},{4,0},{6,2},{8,12},{10,14},{12,8},{14,10},{1,5},{3,7},... | collective-permute-start | bytes 393224 | tf_op jit(solution)/shard_map/ppermute | solution.py:504
  20.5 3.5 %collective-permute-done.2.refs_1_ = f32[2,256,128]{2,1,0:T(8,128)S(1)} collective-permute-done((f32[2,256,128]{2,1,0:T(8,128)S(1)}, f32[2,256,128]{2,1,0:T(8,128)S(1)}, u32[]{:S(2)}, u32[]{:S(2)}) %collective-permute-start.2) | collective-permute-done | bytes 262176 | tf_op jit(solution)/shard_map/ppermute | solution.py:504
  23.9 0.3 join.3
  24.2 1.7 %collective-permute-start.3 = (f32[1,256,128]{2,1,0:T(8,128)S(1)}, f32[1,256,128]{2,1,0:T(8,128)S(1)}, u32[]{:S(2)}, u32[]{:S(2)}) collective-permute-start(f32[1,256,128]{2,1,0:T(8,128)S(1)} %get-tuple-element.28), channel_id=1, source_target_pairs={{0,4},{2,6},{4,0},{6,2},{8,12},{10,14},{12,8},{14,10},{1,5},{3,7},... | collective-permute-start | bytes 393224 | tf_op jit(solution)/shard_map/ppermute | solution.py:504
  26.0 3.1 %new_token.1.refs_2_.refs_4_ = f32[2,4,8,128]{3,2,1,0:T(8,128)S(1)} custom-call(bf16[2,2048]{1,0:T(2,128)(2,1)S(1)} %copy-done.6, bf16[2048,512]{1,0:T(8,128)(2,1)S(1)} %copy-done, bf16[2048,512]{1,0:T(8,128)(2,1)S(1)} %copy-done.1, bf16[2048,512]{1,0:T(8,128)(2,1)S(1)} %copy-done.3, bf16[8,2048]{1,0:T(8,128)(2,1)S(1)} %bitcast.8, ...), custom_call_target="tpu_custom_call" | custom-call | tf_op jit(solution)/shard_map/new_token/pallas_call | solution.py:305
  29.1 0.4 pack.2
  29.5 2.6 %collective-permute-start.4 = (f32[1,136,128]{2,1,0:T(8,128)S(1)}, f32[1,136,128]{2,1,0:T(8,128)S(1)}, u32[]{:S(2)}, u32[]{:S(2)}) collective-permute-start(f32[1,136,128]{2,1,0:T(8,128)S(1)} %get-tuple-element.30), channel_id=1, source_target_pairs={{0,8},{2,10},{4,12},{6,14},{8,0},{10,2},{12,4},{14,6},{1,9},{3,11}... | collective-permute-start | bytes 208904 | tf_op jit(solution)/shard_map/ppermute | solution.py:504
  32.1 0.4 pack.3
  32.4 0.3 collective-permute-start.5
  32.8 3.9 %collective-permute-done.4.refs_2_ = f32[1,136,128]{2,1,0:T(8,128)S(1)} collective-permute-done((f32[1,136,128]{2,1,0:T(8,128)S(1)}, f32[1,136,128]{2,1,0:T(8,128)S(1)}, u32[]{:S(2)}, u32[]{:S(2)}) %collective-permute-start.4) | collective-permute-done | bytes 69664 | tf_op jit(solution)/shard_map/ppermute | solution.py:504
  36.7 1.6 %collective-permute-done.5.refs_3_ = f32[1,136,128]{2,1,0:T(8,128)S(1)} collective-permute-done((f32[1,136,128]{2,1,0:T(8,128)S(1)}, f32[1,136,128]{2,1,0:T(8,128)S(1)}, u32[]{:S(2)}, u32[]{:S(2)}) %collective-permute-start.5) | collective-permute-done | bytes 69664 | tf_op jit(solution)/shard_map/ppermute | solution.py:504
  38.3 0.3 finish.1
  38.6 1.6 %collective-permute-start.6 = (f32[40,128]{1,0:T(8,128)S(1)}, f32[40,128]{1,0:T(8,128)S(1)}, u32[]{:S(2)}, u32[]{:S(2)}) collective-permute-start(f32[40,128]{1,0:T(8,128)S(1)} %get-tuple-element.33), channel_id=1, source_target_pairs={{0,2},{2,0},{4,6},{6,4},{8,10},{10,8},{12,14},{14,12},{1,3},{3,1},... | collective-permute-start | bytes 61448 | tf_op jit(solution)/shard_map/ppermute | solution.py:504
  40.2 2.0 %collective-permute-start.8 = (f32[40,128]{1,0:T(8,128)S(1)}, f32[40,128]{1,0:T(8,128)S(1)}, u32[]{:S(2)}, u32[]{:S(2)}) collective-permute-start(f32[40,128]{1,0:T(8,128)S(1)} %get-tuple-element.35), channel_id=1, source_target_pairs={{0,6},{2,4},{4,2},{6,0},{8,14},{10,12},{12,10},{14,8},{1,7},{3,5},... | collective-permute-start | bytes 61448 | tf_op jit(solution)/shard_map/ppermute | solution.py:504
  42.2 0.3 collective-permute-done.6.refs_1_
  42.4 1.5 %collective-permute-done.7.refs_2_ = f32[40,128]{1,0:T(8,128)S(1)} collective-permute-done((f32[40,128]{1,0:T(8,128)S(1)}, f32[40,128]{1,0:T(8,128)S(1)}, u32[]{:S(2)}, u32[]{:S(2)}) %collective-permute-start.7) | collective-permute-done | bytes 20512 | tf_op jit(solution)/shard_map/ppermute | solution.py:504
  44.0 0.9 %collective-permute-done.8.refs_3_ = f32[40,128]{1,0:T(8,128)S(1)} collective-permute-done((f32[40,128]{1,0:T(8,128)S(1)}, f32[40,128]{1,0:T(8,128)S(1)}, u32[]{:S(2)}, u32[]{:S(2)}) %collective-permute-start.8) | collective-permute-done | bytes 20512 | tf_op jit(solution)/shard_map/ppermute | solution.py:504
  44.9 0.6 %place_outputs.1 = (bf16[2,4,16,128]{3,2,1,0:T(8,128)(2,1)}, bf16[2,512]{1,0:T(2,128)(2,1)}) custom-call(f32[40,128]{1,0:T(8,128)S(1)} %get-tuple-element.32.refs_0_, f32[40,128]{1,0:T(8,128)S(1)} %collective-permute-done.6.refs_1_, f32[40,128]{1,0:T(8,128)S(1)} %collective-permute-done.7.refs_2_, f32[40,128]{1,0:T(8,128)S(1)} %collective-permute-done.8.refs_3_), custom_call_target="tpu_custom_call" | custom-call | tf_op jit(solution)/shard_map/place_outputs/pallas_call | solution.py:475
  (23 shorter events, 0.1 us)
Async XLA Ops:
  0.6 11.2 %copy-start = (bf16[2048,512]{1,0:T(8,128)(2,1)S(1)}, bf16[2048,512]{1,0:T(8,128)(2,1)}, u32[]{:S(2)}) copy-start(bf16[2048,512]{1,0:T(8,128)(2,1)} %refs_1_.3) | copy-start | bytes 6291460
  0.6 11.2 %copy-start.1 = (bf16[2048,512]{1,0:T(8,128)(2,1)S(1)}, bf16[2048,512]{1,0:T(8,128)(2,1)}, u32[]{:S(2)}) copy-start(bf16[2048,512]{1,0:T(8,128)(2,1)} %refs_2_.3) | copy-start | bytes 6291460
  0.7 11.2 %copy-start.2 = (bf16[2,256,2048]{2,1,0:T(8,128)(2,1)S(1)}, bf16[2,256,2048]{2,1,0:T(8,128)(2,1)}, u32[]{:S(2)}) copy-start(bf16[2,256,2048]{2,1,0:T(8,128)(2,1)} %refs_0_.3) | copy-start | bytes 6291460
  8.8 9.8 %collective-permute-start = (f32[2,256,128]{2,1,0:T(8,128)S(1)}, f32[2,256,128]{2,1,0:T(8,128)S(1)}, u32[]{:S(2)}, u32[]{:S(2)}) collective-permute-start(f32[2,256,128]{2,1,0:T(8,128)S(1)} %get-tuple-element.20), channel_id=1, source_target_pairs={{0,2},{2,0},{4,6},{6,4},{8,10},{10,8},{12,14},{14,12},{1,3},{3,1},... | collective-permute-start | bytes 786440 | tf_op jit(solution)/shard_map/ppermute | solution.py:504
  11.9 14.1 %copy-start.3 = (bf16[2048,512]{1,0:T(8,128)(2,1)S(1)}, bf16[2048,512]{1,0:T(8,128)(2,1)}, u32[]{:S(2)}) copy-start(bf16[2048,512]{1,0:T(8,128)(2,1)} %wq_ref.1) | copy-start | bytes 6291460
  11.9 14.1 %copy-start.4 = (bf16[2048,8]{0,1:T(8,128)(2,1)S(1)}, bf16[2048,8]{0,1:T(8,128)(2,1)}, u32[]{:S(2)}) copy-start(bf16[2048,8]{0,1:T(8,128)(2,1)} %param.16) | copy-start | bytes 98308
  11.9 14.1 %copy-start.5 = (bf16[2048,8]{0,1:T(8,128)(2,1)S(1)}, bf16[2048,8]{0,1:T(8,128)(2,1)}, u32[]{:S(2)}) copy-start(bf16[2048,8]{0,1:T(8,128)(2,1)} %param.17) | copy-start | bytes 98308
  11.9 14.1 %copy-start.6 = (bf16[2,2048]{1,0:T(2,128)(2,1)S(1)}, bf16[2,2048]{1,0:T(2,128)(2,1)}, u32[]{:S(2)}) copy-start(bf16[2,2048]{1,0:T(2,128)(2,1)} %x_ref.1) | copy-start | bytes 24580
  11.9 14.0 %copy-start.7 = (f32[4]{0:T(128)S(1)}, f32[4]{0:T(128)}, u32[]{:S(2)}) copy-start(f32[4]{0:T(128)} %param.18) | copy-start | bytes 52
  11.9 14.0 %copy-start.8 = (f32[4]{0:T(128)S(1)}, f32[4]{0:T(128)}, u32[]{:S(2)}) copy-start(f32[4]{0:T(128)} %param.19) | copy-start | bytes 52
  16.1 7.8 %collective-permute-start.2 = (f32[2,256,128]{2,1,0:T(8,128)S(1)}, f32[2,256,128]{2,1,0:T(8,128)S(1)}, u32[]{:S(2)}, u32[]{:S(2)}) collective-permute-start(f32[2,256,128]{2,1,0:T(8,128)S(1)} %get-tuple-element.26), channel_id=1, source_target_pairs={{0,2},{2,0},{4,6},{6,4},{8,10},{10,8},{12,14},{14,12},{1,3},{3,1},... | collective-permute-start | bytes 786440 | tf_op jit(solution)/shard_map/ppermute | solution.py:504
  18.9 10.2 %collective-permute-start.1 = (f32[1,256,128]{2,1,0:T(8,128)S(1)}, f32[1,256,128]{2,1,0:T(8,128)S(1)}, u32[]{:S(2)}, u32[]{:S(2)}) collective-permute-start(f32[1,256,128]{2,1,0:T(8,128)S(1)} %get-tuple-element.22), channel_id=1, source_target_pairs={{0,4},{2,6},{4,0},{6,2},{8,12},{10,14},{12,8},{14,10},{1,5},{3,7},... | collective-permute-start | bytes 393224 | tf_op jit(solution)/shard_map/ppermute | solution.py:504
  24.2 14.1 %copy-start.9 = (f32[128]{0:T(128)S(1)}, f32[128]{0:T(128)}, u32[]{:S(2)}) copy-start(f32[128]{0:T(128)} %param.23) | copy-start | bytes 1540
  24.2 7.8 %collective-permute-start.3 = (f32[1,256,128]{2,1,0:T(8,128)S(1)}, f32[1,256,128]{2,1,0:T(8,128)S(1)}, u32[]{:S(2)}, u32[]{:S(2)}) collective-permute-start(f32[1,256,128]{2,1,0:T(8,128)S(1)} %get-tuple-element.28), channel_id=1, source_target_pairs={{0,4},{2,6},{4,0},{6,2},{8,12},{10,14},{12,8},{14,10},{1,5},{3,7},... | collective-permute-start | bytes 393224 | tf_op jit(solution)/shard_map/ppermute | solution.py:504
  29.5 7.2 %collective-permute-start.4 = (f32[1,136,128]{2,1,0:T(8,128)S(1)}, f32[1,136,128]{2,1,0:T(8,128)S(1)}, u32[]{:S(2)}, u32[]{:S(2)}) collective-permute-start(f32[1,136,128]{2,1,0:T(8,128)S(1)} %get-tuple-element.30), channel_id=1, source_target_pairs={{0,8},{2,10},{4,12},{6,14},{8,0},{10,2},{12,4},{14,6},{1,9},{3,11}... | collective-permute-start | bytes 208904 | tf_op jit(solution)/shard_map/ppermute | solution.py:504
  32.4 5.9 %collective-permute-start.5 = (f32[1,136,128]{2,1,0:T(8,128)S(1)}, f32[1,136,128]{2,1,0:T(8,128)S(1)}, u32[]{:S(2)}, u32[]{:S(2)}) collective-permute-start(f32[1,136,128]{2,1,0:T(8,128)S(1)} %get-tuple-element.31), channel_id=1, source_target_pairs={{0,8},{2,10},{4,12},{6,14},{8,0},{10,2},{12,4},{14,6},{1,9},{3,11}... | collective-permute-start | bytes 208904 | tf_op jit(solution)/shard_map/ppermute | solution.py:504
  38.6 3.8 %collective-permute-start.6 = (f32[40,128]{1,0:T(8,128)S(1)}, f32[40,128]{1,0:T(8,128)S(1)}, u32[]{:S(2)}, u32[]{:S(2)}) collective-permute-start(f32[40,128]{1,0:T(8,128)S(1)} %get-tuple-element.33), channel_id=1, source_target_pairs={{0,2},{2,0},{4,6},{6,4},{8,10},{10,8},{12,14},{14,12},{1,3},{3,1},... | collective-permute-start | bytes 61448 | tf_op jit(solution)/shard_map/ppermute | solution.py:504
  40.2 3.8 %collective-permute-start.7 = (f32[40,128]{1,0:T(8,128)S(1)}, f32[40,128]{1,0:T(8,128)S(1)}, u32[]{:S(2)}, u32[]{:S(2)}) collective-permute-start(f32[40,128]{1,0:T(8,128)S(1)} %get-tuple-element.34), channel_id=1, source_target_pairs={{0,4},{2,6},{4,0},{6,2},{8,12},{10,14},{12,8},{14,10},{1,5},{3,7},... | collective-permute-start | bytes 61448 | tf_op jit(solution)/shard_map/ppermute | solution.py:504
  40.2 4.7 %collective-permute-start.8 = (f32[40,128]{1,0:T(8,128)S(1)}, f32[40,128]{1,0:T(8,128)S(1)}, u32[]{:S(2)}, u32[]{:S(2)}) collective-permute-start(f32[40,128]{1,0:T(8,128)S(1)} %get-tuple-element.35), channel_id=1, source_target_pairs={{0,6},{2,4},{4,2},{6,0},{8,14},{10,12},{12,10},{14,8},{1,7},{3,5},... | collective-permute-start | bytes 61448 | tf_op jit(solution)/shard_map/ppermute | solution.py:504

commit v2 on v1

v2 whole, which is shorter than its diff:
```python
import jax
import jax.numpy as jnp
from jax import lax
from jax.experimental import pallas as pl
from jax.experimental.pallas import tpu as pltpu
from jax.sharding import PartitionSpec as P


EPS = 1e-06
CHUNK = 128
PAD = 8
F32 = jnp.float32
BF16 = jnp.bfloat16
WHOLE = pl.BlockSpec(memory_space=pltpu.VMEM)
LIMIT = pltpu.CompilerParams(vmem_limit_bytes=16 * 2**20)


def dot(a, b):
    return jnp.dot(a, b, preferred_element_type=F32)


def dot_nt(a, b):
    return lax.dot_general(a, b, (((1,), (1,)), ((), ())), preferred_element_type=F32)


def dot_tn(a, b):
    return lax.dot_general(a, b, (((0,), (0,)), ((), ())), preferred_element_type=F32)


def halves(a):
    high = a.astype(BF16)
    return high, (a - high.astype(F32)).astype(BF16)


def dot3(a, b):
    ah, al = halves(a)
    bh, bl = halves(b)
    return dot(ah, bh) + dot(ah, bl) + dot(al, bh)


def silu(values):
    return values * jax.nn.sigmoid(values)


def unit(values):
    return values * lax.rsqrt(jnp.sum(values * values, axis=-1, keepdims=True) + EPS)


def softplus(values):
    return jnp.maximum(values, 0.0) + jnp.log1p(jnp.exp(-jnp.abs(values)))


def pick_lane(values, lane):
    places = lax.broadcasted_iota(jnp.int32, values.shape, 1)
    return jnp.sum(jnp.where(places == lane, values, 0.0), axis=1, keepdims=True)


def gate_tables(x, wd, ws, speeds, ceilings, mult, spike, heads, upper):
    total = wd.shape[0]
    rates = jnp.concatenate([wd.astype(F32), ws.astype(F32)], axis=0)
    both = dot_nt(rates.astype(BF16), x)
    shard = lax.axis_index("tp")
    row = lax.broadcasted_iota(jnp.int32, (heads, heads), 0)
    col = lax.broadcasted_iota(jnp.int32, (heads, heads), 1)

    def mine(full):
        part = full[:heads]
        for t in range(1, total // heads):
            part = jnp.where(shard == t, full[t * heads : (t + 1) * heads], part)
        return part

    def upright(values):
        return jnp.sum(jnp.where(row == col, values[:, :heads], 0.0), axis=1, keepdims=True)

    gates = -upright(speeds) * softplus(mine(both[:total])) * mult + spike
    beta = upright(ceilings) * jax.nn.sigmoid(mine(both[total:]))
    rows = []
    for c in range(x.shape[0] // CHUNK):
        lanes = slice(c * CHUNK, (c + 1) * CHUNK)
        rows.append(beta[:, lanes])
        rows.append(
            jnp.dot(gates[:, lanes], upper, precision=lax.Precision.HIGHEST, preferred_element_type=F32)
        )
    fill = -sum(r.shape[0] for r in rows) % PAD
    if fill:
        rows.append(jnp.zeros((fill, CHUNK), F32))
    return jnp.concatenate(rows, axis=0)


def local_maps_kernel(*refs, heads, own_heads, first, bits):
    targets = 2**bits
    if first:
        x_hbm, wk_hbm, wv_hbm = refs[:3]
        small_hbm = refs[3:9]
        table_ref, x_s, w_s = refs[9:12]
        rest = refs[12:]
    else:
        x_s, w_s, table_ref = refs[:3]
        rest = refs[3:]
    outs, rest = rest[:targets], rest[targets:]
    k_s, v_s, lower_s, inverse_s, half_s, mask_s, map_s = rest[:7]
    small_s, sems = rest[7:-1], rest[-1]
    seqs, span, width = x_s.shape
    dim = k_s.shape[-1]
    count = seqs * span
    chunks = count // CHUNK
    group = len(own_heads)
    steps = [2**i for i in range(CHUNK.bit_length() - 1)]

    if first:
        copies = [pltpu.make_async_copy(x_hbm.at[s], x_s.at[s], sems.at[s]) for s in range(seqs)]
        for i, (source, target) in enumerate(zip(small_hbm, small_s)):
            copies.append(pltpu.make_async_copy(source, target, sems.at[seqs + i]))
        base = len(copies)
        for h in range(heads):
            for i, w_hbm in enumerate((wk_hbm, wv_hbm)):
                copies.append(
                    pltpu.make_async_copy(
                        w_hbm.at[:, pl.ds(h * dim, dim)],
                        w_s.at[h, :, pl.ds(i * dim, dim)],
                        sems.at[base + 2 * h + i],
                    )
                )
        for copy in copies:
            copy.start()

    row = lax.broadcasted_iota(jnp.int32, (CHUNK, CHUNK), 0)
    col = lax.broadcasted_iota(jnp.int32, (CHUNK, CHUNK), 1)
    strict = row > col
    eye = jnp.where(row == col, 1.0, 0.0)

    def level(m):
        return (row // (2 * m) == col // (2 * m)) & (row // m != col // m)

    for i, m in enumerate(steps):
        mask_s[i] = jnp.where(level(m), 1.0, 0.0).astype(BF16)
    mask_s[len(steps)] = jnp.where(strict, 1.0, 0.0).astype(BF16)

    if first:
        for copy in copies[:base]:
            copy.wait()
    flat = x_s[...].reshape(count, width)
    if first:
        wd, ws, speeds, ceilings = (ref[...] for ref in small_s[:4])
        mult, spike = (
            jnp.concatenate([ref[s] for s in range(seqs)], axis=1) for ref in small_s[4:]
        )
        table_ref[...] = gate_tables(
            flat, wd, ws, speeds, ceilings, mult, spike, heads, jnp.where(row <= col, 1.0, 0.0)
        )
    columns = table_ref[...].T

    def at(c, g, which):
        return (2 * c + which) * heads + own_heads[g]

    def column(c, g, which):
        return jnp.broadcast_to(columns[:, at(c, g, which) : at(c, g, which) + 1], (CHUNK, CHUNK))

    pieces = [(g, c) for g in range(group) for c in range(chunks)]

    for g, h in enumerate(own_heads):
        if first:
            copies[base + 2 * h].wait()
            copies[base + 2 * h + 1].wait()
        raw = dot(flat, w_s[h]).astype(BF16).astype(F32)
        k_s[g] = unit(silu(raw[:, :dim]))
        v_s[g] = silu(raw[:, dim:])

    def rows_of(c):
        return slice(c * CHUNK, (c + 1) * CHUNK)

    for n, (g, c) in enumerate(pieces):
        short = k_s[g, rows_of(c)].astype(BF16)
        gram = dot_nt(short, short)
        place = at(c, g, 1)
        spread = jnp.exp(jnp.minimum(column(c, g, 1) - table_ref[place : place + 1, :], 0.0))
        lower = jnp.where(strict, gram * column(c, g, 0) * spread, 0.0)
        lower_s[n] = lower.astype(BF16)
        inverse_s[n] = (eye - jnp.where(level(1), lower, 0.0)).astype(BF16)

    for i, m in list(enumerate(steps))[1:]:
        odd = [slice(o, o + m) for o in range(m, CHUNK, 2 * m)]
        if m < 16:
            for n in range(len(pieces)):
                half_s[n] = dot(inverse_s[n], lower_s[n] * mask_s[i]).astype(BF16)
            for n in range(len(pieces)):
                inverse_s[n] = inverse_s[n] - dot(half_s[n], inverse_s[n]).astype(BF16)
        else:
            for n in range(len(pieces)):
                picked = jnp.concatenate([inverse_s[n, o] for o in odd], axis=0)
                half_s[n, : CHUNK // 2] = dot(picked, lower_s[n] * mask_s[i]).astype(BF16)
            for n in range(len(pieces)):
                change = dot(half_s[n, : CHUNK // 2], inverse_s[n]).astype(BF16)
                for j, o in enumerate(odd):
                    inverse_s[n, o] = inverse_s[n, o] - change[j * m : (j + 1) * m]

    terms = []
    for n, (g, c) in enumerate(pieces):
        keys, values = k_s[g, rows_of(c)], v_s[g, rows_of(c)]
        strength, total_log = column(c, g, 0), column(c, g, 1)
        last = total_log[CHUNK - 1 : CHUNK]
        off = inverse_s[n] * mask_s[len(steps)]
        source = jnp.concatenate([keys * (strength * jnp.exp(total_log)), values * strength], axis=1)
        solved = source + dot(off, source.astype(BF16))
        faded = (keys * jnp.exp(last - total_log)).astype(BF16)
        change = dot_tn(faded, solved.astype(BF16))
        terms.append((change[:, :dim], change[:, dim:], jnp.exp(last)))

    per = chunks // seqs
    for g in range(group):
        for s in range(seqs):
            mine = terms[g * chunks + s * per : g * chunks + (s + 1) * per]
            eraser, target, decay = mine[0]
            held_a, held_b = decay * eye - eraser, target
            for eraser, target, decay in mine[1:]:
                change = dot(
                    eraser.astype(BF16), jnp.concatenate([held_a, held_b], axis=1).astype(BF16)
                )
                held_a = decay * held_a - change[:, :dim]
                held_b = decay * held_b - change[:, dim:] + target
            map_s[s * group + g, :dim, :] = held_a
            map_s[s * group + g, dim:, :] = held_b
    states = seqs * group >> bits
    place = lax.axis_index("sp")
    for mask, out in enumerate(outs):
        for i in range(states):
            out[i] = map_s[state_index(i, place ^ mask, seqs * group, bits)]
    if first:
        for copy in copies[base + 2 * len(own_heads) :]:
            copy.wait()


def local_maps(x, w, small, heads, own_heads, dim, bits, table=None):
    seqs, span, width = x.shape
    count = seqs * span
    group = len(own_heads)
    pieces = group * count // CHUNK
    square = (CHUNK, CHUNK)
    results = [pltpu.VMEM((seqs * group >> bits, 2 * dim, dim), F32)] * 2**bits
    scratch = [
        pltpu.VMEM((group, count, dim), F32),
        pltpu.VMEM((group, count, dim), F32),
        pltpu.VMEM((pieces,) + square, BF16),
        pltpu.VMEM((pieces,) + square, BF16),
        pltpu.VMEM((pieces,) + square, BF16),
        pltpu.VMEM((CHUNK.bit_length(),) + square, BF16),
        pltpu.VMEM((seqs * group, 2 * dim, dim), F32),
    ]
    first = table is None
    if first:
        rows = -(-2 * heads * (count // CHUNK) // PAD) * PAD
        scratch += [pltpu.VMEM(a.shape, a.dtype) for a in small]
        operands = [pltpu.with_memory_space_constraint(a, pltpu.HBM) for a in (x, *w, *small)]
        in_specs = [pl.BlockSpec(memory_space=pltpu.HBM)] * len(operands)
        results = [
            pltpu.VMEM((rows, CHUNK), F32),
            pltpu.VMEM(x.shape, BF16),
            pltpu.VMEM((heads, width, 2 * dim), BF16),
        ] + results
    else:
        operands = [x, w, table]
        in_specs = [WHOLE] * 3
    scratch.append(pltpu.SemaphoreType.DMA((seqs + len(small) + 2 * heads,)))
    return pl.pallas_call(
        lambda *refs: local_maps_kernel(
            *refs, heads=heads, own_heads=own_heads, first=first, bits=bits
        ),
        in_specs=in_specs,
        out_specs=[WHOLE] * len(results),
        out_shape=results,
        scratch_shapes=scratch,
        compiler_params=pltpu.CompilerParams(vmem_limit_bytes=24 * 2**20),
        name="local_maps",
    )(*operands)


def state_index(index, place, states, bits):
    base = index
    for b in range(bits):
        states //= 2
        base = base + ((place >> b) % 2) * states
    return base


def new_token_kernel(
    x_ref, w_ref, wq_ref, wd_ref, ws_ref, speed_ref, ceil_ref, out_ref, *, groups, bits
):
    seqs, _ = x_ref.shape
    dim = w_ref.shape[2] // 2
    heads = w_ref.shape[0]
    states = seqs * len(groups[0]) >> bits
    place = lax.axis_index("sp")
    x = x_ref[...]
    decay_pre = dot_nt(x, wd_ref[...])
    strength_pre = dot_nt(x, ws_ref[...])
    for g, own_heads in enumerate(groups):
        for i in range(states):
            index = state_index(i, place, seqs * len(own_heads), bits)
            s, head = index // len(own_heads), index % len(own_heads) + own_heads[0]
            lane = lax.axis_index("tp") * heads + head
            raw = dot(x, w_ref[head]).astype(BF16).astype(F32)
            lanes = pl.ds(pl.multiple_of(head * dim, dim), dim)
            query_raw = dot(x, wq_ref[:, lanes]).astype(BF16).astype(F32)
            query = unit(silu(query_raw)) * dim ** (-0.5)
            keys = unit(silu(raw[:, :dim]))
            values = silu(raw[:, dim:])
            fading = jnp.exp(
                -pick_lane(speed_ref[:, :heads], head) * softplus(pick_lane(decay_pre, lane))
            )
            match = jnp.sum(query * keys, axis=-1, keepdims=True) * (
                pick_lane(ceil_ref[:, :heads], head) * jax.nn.sigmoid(pick_lane(strength_pre, lane))
            )
            wide = [jnp.broadcast_to(item, query.shape) for item in (fading, match)]
            for n, item in enumerate([query, keys, values, *wide]):
                chosen = item[:1]
                for t in range(1, seqs):
                    chosen = jnp.where(s == t, item[t : t + 1], chosen)
                out_ref[g * states + i, n : n + 1, :] = chosen


def new_token(x, w, wq, small, groups, bits, dim):
    states = x.shape[0] * len(groups[0]) >> bits
    return pl.pallas_call(
        lambda *refs: new_token_kernel(*refs, groups=groups, bits=bits),
        in_specs=[WHOLE] * 7,
        out_specs=WHOLE,
        out_shape=pltpu.VMEM((states * len(groups), PAD, dim), F32),
        compiler_params=LIMIT,
        name="new_token",
    )(x, w, wq, *small[:4])


def compose(early, late, dim):
    early = jnp.concatenate([early[:dim], early[dim:]], axis=1)
    both = dot3(late[:dim], early)
    return jnp.concatenate([both[:, :dim], both[:, dim:] + late[dim:]], axis=0)


def gathered(refs, order_s, i, low, dim):
    place = lax.axis_index("sp") >> low
    count = len(refs)
    for mask, ref in enumerate(refs):
        order_s[(place % count) ^ mask] = ref[i]
    held = [order_s[n] for n in range(count)]
    while len(held) > 1:
        held = [compose(held[n], held[n + 1], dim) for n in range(0, len(held), 2)]
    return held[0]


def merge_kernel(*refs, low):
    ins, out, order_s = refs[:-2], refs[-2], refs[-1]
    for i in range(out.shape[0]):
        out[i] = gathered(ins, order_s, i, low, out.shape[2])


def merge(parts, low):
    shape = parts[0].shape
    return pl.pallas_call(
        lambda *refs: merge_kernel(*refs, low=low),
        in_specs=[WHOLE] * len(parts),
        out_specs=WHOLE,
        out_shape=pltpu.VMEM(shape, F32),
        scratch_shapes=[pltpu.VMEM((len(parts),) + shape[1:], F32)],
        compiler_params=LIMIT,
        name="merge",
    )(*parts)


def pack_kernel(*refs, count, earlier, low, top, last):
    ins, rest = refs[:count], refs[count:]
    befores, rest = rest[:earlier], rest[earlier:]
    if last:
        token_ref, own_ref, send_ref, order_s = rest
    else:
        own_ref, send_ref, full_ref, order_s = rest
    states, _, dim = ins[0].shape
    right = (lax.axis_index("sp") >> top) % 2 == 1
    half = dim // 2
    fulls = []
    for i in range(states):
        full = gathered(ins, order_s, i, low, dim)
        fulls.append(full)
        out_a, out_b = full[:dim], full[dim:]
        at = i * dim
        own_ref[at : at + half, :] = jnp.where(right, out_a[half:], out_b[:half])
        own_ref[at + half : at + dim, :] = out_b[half:]
        send_ref[at : at + half, :] = jnp.where(right, out_a[:half], out_b[:half])
        send_ref[at + half : at + dim, :] = jnp.where(right, out_b[:half], out_b[half:])
        if not last:
            full_ref[i] = full
    if last:
        everything = [ref[i] for ref in befores for i in range(states)] + fulls
        for n, full in enumerate(everything):
            token = token_ref[n]
            reads = dot3(token, jnp.concatenate([full[:dim], full[dim:]], axis=1))
            tail = jnp.concatenate([reads[:2, :dim], reads[:2, dim:]], axis=0)
            at = states * dim + 4 * n
            own_ref[at : at + 4, :] = tail
            send_ref[at : at + 4, :] = tail


def pack(parts, befores, token, low, top):
    states, rows, dim = parts[0].shape
    last = token is not None
    tail = -(-4 * states * (len(befores) + 1) // PAD) * PAD if last else 0
    shape = pltpu.VMEM((states * dim + tail, dim), F32)
    results = [shape, shape] + ([] if last else [pltpu.VMEM(parts[0].shape, F32)])
    operands = [*parts, *befores] + ([token] if last else [])
    return pl.pallas_call(
        lambda *refs: pack_kernel(
            *refs, count=len(parts), earlier=len(befores), low=low, top=top, last=last
        ),
        in_specs=[WHOLE] * len(operands),
        out_specs=[WHOLE] * len(results),
        out_shape=results,
        scratch_shapes=[pltpu.VMEM((len(parts), rows, dim), F32)],
        compiler_params=LIMIT,
        name="pack",
    )(*operands)


def finish_kernel(*refs, count, states, top, block):
    owns, gots = refs[:count], refs[count : 2 * count]
    token_ref, gain_ref = refs[2 * count : 2 * count + 2]
    outs, rows_s = refs[2 * count + 2 : -1], refs[-1]
    dim = gain_ref.shape[1]
    place = lax.axis_index("sp")
    right = (place >> top) % 2 == 1
    half = dim // 2
    reads = []
    total = count * states
    for n in range(total):
        at = n % states * dim
        own, got = owns[n // states][at : at + dim, :], gots[n // states][at : at + dim, :]
        state = jnp.where(right, got, own)
        later = jnp.where(right, own, got)
        at = states * dim + 4 * n
        tail = jnp.where(right, owns[-1][at : at + 4, :], gots[-1][at : at + 4, :])
        full = dot3(jnp.concatenate([later[:half], tail, tail], axis=0), state)
        rows_s[n] = full[:half] + later[half:]
        seen = full[half : half + 2] + tail[2:]
        token = token_ref[n]
        fading, match = token[3:4], token[4:5]
        mixed = fading * (seen[:1] - match * seen[1:2]) + match * token[2:3]
        scale = lax.rsqrt(jnp.mean(mixed * mixed, axis=-1, keepdims=True) + EPS)
        reads.append(mixed * scale * gain_ref[...])
    blocks = half // block
    for mask, out in enumerate(outs):
        start = ((place ^ mask) % blocks) * block
        for n in range(total):
            out[n * block : (n + 1) * block, :] = rows_s[n, pl.ds(start, block), :]
            out[total * block + n : total * block + n + 1, :] = reads[n]


def finish(owns, gots, token, gain, top, bits, block):
    dim = owns[0].shape[1]
    total = token.shape[0]
    states = total // len(owns)
    rows = -(-(total * block + total) // PAD) * PAD
    return pl.pallas_call(
        lambda *refs: finish_kernel(*refs, count=len(owns), states=states, top=top, block=block),
        in_specs=[WHOLE] * (2 * len(owns) + 2),
        out_specs=[WHOLE] * 2**bits,
        out_shape=[pltpu.VMEM((rows, dim), F32)] * 2**bits,
        scratch_shapes=[pltpu.VMEM((total, dim // 2, dim), F32)],
        compiler_params=LIMIT,
        name="finish",
    )(*owns, *gots, token, gain.reshape(1, -1))


def place_kernel(*refs, groups, bits, block):
    count = 2**bits
    ins, cache_ref, read_ref, reads_s = refs[:count], refs[count], refs[count + 1], refs[count + 2]
    seqs, heads, _, dim = cache_ref.shape
    total = seqs * heads // count
    states = total // len(groups)
    place = lax.axis_index("sp")
    for mask, got in enumerate(ins):
        for g, own_heads in enumerate(groups):
            for i in range(states):
                index = state_index(i, place ^ mask, seqs * len(own_heads), bits)
                s, h = index // len(own_heads), index % len(own_heads) + own_heads[0]
                n = g * states + i
                cache_ref[s, h] = got[n * block : (n + 1) * block, :].astype(BF16)
                reads_s[pl.ds(s * heads + h, 1), :] = got[total * block + n : total * block + n + 1, :]
    for h in range(heads):
        rows = [reads_s[s * heads + h : s * heads + h + 1, :] for s in range(seqs)]
        read_ref[:, h * dim : (h + 1) * dim] = jnp.concatenate(rows, axis=0).astype(BF16)


def place_outputs(parts, groups, seqs, heads, dim, block, bits):
    return pl.pallas_call(
        lambda *refs: place_kernel(*refs, groups=groups, bits=bits, block=block),
        in_specs=[WHOLE] * len(parts),
        out_specs=[WHOLE] * 2,
        out_shape=[
            jax.ShapeDtypeStruct((seqs, heads, block, dim), BF16),
            jax.ShapeDtypeStruct((seqs, heads * dim), BF16),
        ],
        scratch_shapes=[pltpu.VMEM((seqs * heads, dim), F32)],
        compiler_params=LIMIT,
        name="place_outputs",
    )(*parts)


def on_device(
    prompt_elements, address_weights, content_weights, lookup_weights, forgetting_weights,
    update_intensity_weights, forgetting_speeds, update_intensity_ceiling, forgetting_multiplier,
    spike_offsets, upcoming_element_vector, retrieval_rms_multiplier,
):
    seqs = prompt_elements.shape[0]
    dim = retrieval_rms_multiplier.shape[0]
    heads = forgetting_speeds.shape[0]
    places = lax.axis_size("sp")
    stages = places.bit_length() - 1
    block = dim // places

    def exchange(values, mask):
        got = lax.ppermute(values, "sp", [(i, i ^ mask) for i in range(places)])
        return pltpu.with_memory_space_constraint(got, pltpu.VMEM)

    parts = 2 if heads % 2 == 0 else 1
    size = heads // parts
    groups = [list(range(g * size, (g + 1) * size)) for g in range(parts)]

    def flat_row(values):
        return jnp.concatenate([values] * (2 if heads == 1 else 1)).reshape(1, -1)

    small = (
        forgetting_weights.T, update_intensity_weights.T, flat_row(forgetting_speeds),
        flat_row(update_intensity_ceiling), forgetting_multiplier.transpose(0, 2, 1),
        spike_offsets.transpose(0, 2, 1),
    )
    bits = min((seqs * size).bit_length() - 1, stages - 1)
    top = stages - 1
    table = None
    flows = []
    x, w = prompt_elements, (address_weights, content_weights)
    for own_heads in groups:
        results = local_maps(x, w, small, heads, own_heads, dim, bits, table)
        if table is None:
            table, x, w, *results = results
        flows.append([part if m == 0 else exchange(part, m) for m, part in enumerate(results)])
    token = new_token(upcoming_element_vector, w, lookup_weights, small, groups, bits, dim)
    low, span = 0, bits
    while low + span < top:
        for flow in flows:
            joint = merge(flow, low)
            flow[:] = joint, exchange(joint, 2 ** (low + span))
        low, span = low + span, 1
    owns, gots, fulls = [], [], []
    for g, flow in enumerate(flows):
        last = g == len(flows) - 1
        own, send, *full = pack(flow, fulls if last else [], token if last else None, low, top)
        fulls += full
        owns.append(own)
        gots.append(exchange(send, 2**top))
    pieces = finish(owns, gots, token, retrieval_rms_multiplier, top, bits, block)
    pieces = [piece if mask == 0 else exchange(piece, mask) for mask, piece in enumerate(pieces)]
    return tuple(place_outputs(pieces, groups, seqs, heads, dim, block, bits))


def solution(mesh):
    in_specs = (
        P("gr", "sp", None),
        P(None, "tp"),
        P(None, "tp"),
        P(None, "tp"),
        P(),
        P(),
        P("tp"),
        P("tp"),
        P("gr", "sp", "tp"),
        P("gr", "sp", "tp"),
        P("gr", None),
        P(),
    )
    out_specs = (P("gr", "tp", "sp", None), P("gr", "tp"))

    return jax.shard_map(
        on_device, mesh=mesh, in_specs=in_specs, out_specs=out_specs, check_vma=False
    )
```

time: 45.7 us -> 43.2 us (0.945)
  Pallas kernels: 17.6 us -> 15.3 us
  waiting for transfers between devices: 14.1 us -> 12.3 us
  starting transfers between devices: 13 us -> 14.7 us
    pallas_call x7 -> x5, Pallas kernels: 5.34 us -> 2.95 us  [the longest x2 1.23 us: pack(): pl.pallas_call(lambda *refs: pack_kernel(*refs, count=len(parts), earlier...]
    ppermute x9 -> x11, waiting for transfers between devices: 14.1 us -> 12.3 us  [exchange(): got = lax.ppermute(values, 'sp', [(i, i ^ mask) for i in range(places)])]
    ppermute x9 -> x11, starting transfers between devices: 13 us -> 14.7 us  [exchange(): got = lax.ppermute(values, 'sp', [(i, i ^ mask) for i in range(places)])]
  transfers between devices with their start and end apart: 9 -> 11, of which waited for: 7 -> 7; matrix products, arithmetic and copies ran while one was open for 0% -> 0% of each run, Pallas kernels for 19% -> 13%
where the time goes in v2:
time: 43.2 us; the launch traced here: 43.1 us
  Pallas kernels  15.3 us (35%)
  starting transfers between devices  14.7 us (34%)
  waiting for transfers between devices  12.3 us (28%)
  between operations  0.74 us (2%)
    ppermute x11, starting transfers between devices, exchange(): got = lax.ppermute(values, 'sp', [(i, i ^ mask) for i in range(places)])  14.7 us
    pallas_call x2, Pallas kernels, local_maps(): pl.pallas_call(lambda *refs: local_maps_kernel(*refs, heads=heads, own_he...  12.4 us
    ppermute x11, waiting for transfers between devices, exchange(): got = lax.ppermute(values, 'sp', [(i, i ^ mask) for i in range(places)])  12.3 us
    pallas_call x2, Pallas kernels, pack(): pl.pallas_call(lambda *refs: pack_kernel(*refs, count=len(parts), earlier...  1.23 us
  transfers between devices with their start and end apart: 11, of which 7 were waited for; matrix products, arithmetic and copies ran while one was open for 0% of the time, Pallas kernels for 13%

profile of v2, /device:TPU:0, one launch (start us, length us, event | category | flops | bytes accessed | tf_op | source)
XLA Modules:
  0.0 43.1 jit_solution(15682106591002747035)
XLA Ops:
  0.6 8.1 %local_maps.2 = (f32[32,128]{1,0:T(8,128)S(1)}, bf16[2,256,2048]{2,1,0:T(8,128)(2,1)S(1)}, bf16[4,2048,256]{2,1,0:T(8,128)(2,1)S(1)}, f32[1,256,128]{2,1,0:T(8,1...) custom-call(bf16[2,256,2048]{2,1,0:T(8,128)(2,1)} %refs_0_.2, ...), custom_call_target="tpu_custom_call" | custom-call | tf_op jit(solution)/shard_map/local_maps/pallas_call | solution.py:264
  8.7 3.1 %collective-permute-start = (f32[1,256,128]{2,1,0:T(8,128)S(1)}, f32[1,256,128]{2,1,0:T(8,128)S(1)}, u32[]{:S(2)}, u32[]{:S(2)}) collective-permute-start(f32[1,256,128]{2,1,0:T(8,128)S(1)} %get-tuple-element.23), channel_id=1, source_target_pairs={{0,2},{2,0},{4,6},{6,4},{8,10},{10,8},{12,14},{14,12},{1,3},{3,1},... | collective-permute-start | bytes 393224 | tf_op jit(solution)/shard_map/ppermute | solution.py:519
  11.8 1.6 %collective-permute-start.1 = (f32[1,256,128]{2,1,0:T(8,128)S(1)}, f32[1,256,128]{2,1,0:T(8,128)S(1)}, u32[]{:S(2)}, u32[]{:S(2)}) collective-permute-start(f32[1,256,128]{2,1,0:T(8,128)S(1)} %get-tuple-element.24), channel_id=1, source_target_pairs={{0,4},{2,6},{4,0},{6,2},{8,12},{10,14},{12,8},{14,10},{1,5},{3,7},... | collective-permute-start | bytes 393224 | tf_op jit(solution)/shard_map/ppermute | solution.py:519
  13.4 4.3 %local_maps.3 = (f32[1,256,128]{2,1,0:T(8,128)S(1)}, f32[1,256,128]{2,1,0:T(8,128)S(1)}, f32[1,256,128]{2,1,0:T(8,128)S(1)}, f32[1,256,128]{2,1,0:T(8,128)S(1)}) custom-call(bf16[2,256,2048]{2,1,0:T(8,128)(2,1)S(1)} %get-tuple-element.27.refs_0_, bf16[4,2048,256]{2,1,0:T(8,128)(2,1)S(1)} %get-tuple-element.28.refs_1_, f32[32,128]{1,0:T(8,128)S(1)} %get-tuple-element.29.refs_2_), custom_call_target="tpu_custom_call" | custom-call | tf_op jit(solution)/shard_map/local_maps/pallas_call | solution.py:264
  17.7 2.0 %collective-permute-start.3 = (f32[1,256,128]{2,1,0:T(8,128)S(1)}, f32[1,256,128]{2,1,0:T(8,128)S(1)}, u32[]{:S(2)}, u32[]{:S(2)}) collective-permute-start(f32[1,256,128]{2,1,0:T(8,128)S(1)} %get-tuple-element.31), channel_id=1, source_target_pairs={{0,2},{2,0},{4,6},{6,4},{8,10},{10,8},{12,14},{14,12},{1,3},{3,1},... | collective-permute-start | bytes 393224 | tf_op jit(solution)/shard_map/ppermute | solution.py:519
  19.7 1.6 %collective-permute-start.4 = (f32[1,256,128]{2,1,0:T(8,128)S(1)}, f32[1,256,128]{2,1,0:T(8,128)S(1)}, u32[]{:S(2)}, u32[]{:S(2)}) collective-permute-start(f32[1,256,128]{2,1,0:T(8,128)S(1)} %get-tuple-element.32), channel_id=1, source_target_pairs={{0,4},{2,6},{4,0},{6,2},{8,12},{10,14},{12,8},{14,10},{1,5},{3,7},... | collective-permute-start | bytes 393224 | tf_op jit(solution)/shard_map/ppermute | solution.py:519
  21.3 0.0 collective-permute-start.5
  21.3 0.8 %new_token.1.refs_5_.refs_4_ = f32[2,8,128]{2,1,0:T(8,128)S(1)} custom-call(bf16[2,2048]{1,0:T(2,128)(2,1)S(1)} %copy-done.3, bf16[4,2048,256]{2,1,0:T(8,128)(2,1)S(1)} %get-tuple-element.28.refs_1_, bf16[2048,512]{1,0:T(8,128)(2,1)S(1)} %copy-done, bf16[8,2048]{1,0:T(8,128)(2,1)S(1)} %bitcast.8, bf16[8,2048]{1,0:T(8,128)(2,1)S(1)} %bitcast.10, ...), custom_call_target="tpu_custom_call" | custom-call | tf_op jit(solution)/shard_map/new_token/pallas_call | solution.py:323
  22.1 0.5 %pack.2 = (f32[128,128]{1,0:T(8,128)S(1)}, f32[128,128]{1,0:T(8,128)S(1)}, f32[1,256,128]{2,1,0:T(8,128)S(1)}) custom-call(f32[1,256,128]{2,1,0:T(8,128)S(1)} %get-tuple-element.22.refs_0_, f32[1,256,128]{2,1,0:T(8,128)S(1)} %collective-permute-done.refs_1_, f32[1,256,128]{2,1,0:T(8,128)S(1)} %collective-permute-done.1.refs_2_, ...), custom_call_target="tpu_custom_call" | custom-call | tf_op jit(solution)/shard_map/pack/pallas_call | solution.py:409
  22.7 0.9 %collective-permute-done.3.refs_1_ = f32[1,256,128]{2,1,0:T(8,128)S(1)} collective-permute-done((f32[1,256,128]{2,1,0:T(8,128)S(1)}, f32[1,256,128]{2,1,0:T(8,128)S(1)}, u32[]{:S(2)}, u32[]{:S(2)}) %collective-permute-start.3) | collective-permute-done | bytes 131104 | tf_op jit(solution)/shard_map/ppermute | solution.py:519
  23.6 1.6 %collective-permute-done.4.refs_2_ = f32[1,256,128]{2,1,0:T(8,128)S(1)} collective-permute-done((f32[1,256,128]{2,1,0:T(8,128)S(1)}, f32[1,256,128]{2,1,0:T(8,128)S(1)}, u32[]{:S(2)}, u32[]{:S(2)}) %collective-permute-start.4) | collective-permute-done | bytes 131104 | tf_op jit(solution)/shard_map/ppermute | solution.py:519
  25.2 1.9 %collective-permute-done.5.refs_3_ = f32[1,256,128]{2,1,0:T(8,128)S(1)} collective-permute-done((f32[1,256,128]{2,1,0:T(8,128)S(1)}, f32[1,256,128]{2,1,0:T(8,128)S(1)}, u32[]{:S(2)}, u32[]{:S(2)}) %collective-permute-start.5) | collective-permute-done | bytes 131104 | tf_op jit(solution)/shard_map/ppermute | solution.py:519
  27.1 0.7 %pack.3 = (f32[136,128]{1,0:T(8,128)S(1)}, f32[136,128]{1,0:T(8,128)S(1)}) custom-call(f32[1,256,128]{2,1,0:T(8,128)S(1)} %get-tuple-element.30.refs_0_, f32[1,256,128]{2,1,0:T(8,128)S(1)} %collective-permute-done.3.refs_1_, f32[1,256,128]{2,1,0:T(8,128)S(1)} %collective-permute-done.4.refs_2_, f32[1,256,128]{2,1,0:T(8,128)S(1)} %collective-permute-done.5.refs_3_, ...), custom_call_target="tpu_custom_call" | custom-call | tf_op jit(solution)/shard_map/pack/pallas_call | solution.py:409
  27.8 2.9 %collective-permute-start.7 = (f32[136,128]{1,0:T(8,128)S(1)}, f32[136,128]{1,0:T(8,128)S(1)}, u32[]{:S(2)}, u32[]{:S(2)}) collective-permute-start(f32[136,128]{1,0:T(8,128)S(1)} %get-tuple-element.37), channel_id=1, source_target_pairs={{0,8},{2,10},{4,12},{6,14},{8,0},{10,2},{12,4},{14,6},{1,9},{3,11}... | collective-permute-start | bytes 208904 | tf_op jit(solution)/shard_map/ppermute | solution.py:519
  30.7 0.1 collective-permute-start.6
  30.8 5.8 %collective-permute-done.6.refs_2_ = f32[128,128]{1,0:T(8,128)S(1)} collective-permute-done((f32[128,128]{1,0:T(8,128)S(1)}, f32[128,128]{1,0:T(8,128)S(1)}, u32[]{:S(2)}, u32[]{:S(2)}) %collective-permute-start.6) | collective-permute-done | bytes 65568 | tf_op jit(solution)/shard_map/ppermute | solution.py:519
  36.6 0.3 finish.1
  36.9 1.0 %collective-permute-start.10 = (f32[40,128]{1,0:T(8,128)S(1)}, f32[40,128]{1,0:T(8,128)S(1)}, u32[]{:S(2)}, u32[]{:S(2)}) collective-permute-start(f32[40,128]{1,0:T(8,128)S(1)} %get-tuple-element.41), channel_id=1, source_target_pairs={{0,6},{2,4},{4,2},{6,0},{8,14},{10,12},{12,10},{14,8},{1,7},{3,5},... | collective-permute-start | bytes 61448 | tf_op jit(solution)/shard_map/ppermute | solution.py:519
  37.9 0.7 %collective-permute-start.8 = (f32[40,128]{1,0:T(8,128)S(1)}, f32[40,128]{1,0:T(8,128)S(1)}, u32[]{:S(2)}, u32[]{:S(2)}) collective-permute-start(f32[40,128]{1,0:T(8,128)S(1)} %get-tuple-element.39), channel_id=1, source_target_pairs={{0,2},{2,0},{4,6},{6,4},{8,10},{10,8},{12,14},{14,12},{1,3},{3,1},... | collective-permute-start | bytes 61448 | tf_op jit(solution)/shard_map/ppermute | solution.py:519
  38.6 1.8 %collective-permute-start.9 = (f32[40,128]{1,0:T(8,128)S(1)}, f32[40,128]{1,0:T(8,128)S(1)}, u32[]{:S(2)}, u32[]{:S(2)}) collective-permute-start(f32[40,128]{1,0:T(8,128)S(1)} %get-tuple-element.40), channel_id=1, source_target_pairs={{0,4},{2,6},{4,0},{6,2},{8,12},{10,14},{12,8},{14,10},{1,5},{3,7},... | collective-permute-start | bytes 61448 | tf_op jit(solution)/shard_map/ppermute | solution.py:519
  40.4 1.2 %collective-permute-done.10.refs_3_ = f32[40,128]{1,0:T(8,128)S(1)} collective-permute-done((f32[40,128]{1,0:T(8,128)S(1)}, f32[40,128]{1,0:T(8,128)S(1)}, u32[]{:S(2)}, u32[]{:S(2)}) %collective-permute-start.10) | collective-permute-done | bytes 20512 | tf_op jit(solution)/shard_map/ppermute | solution.py:519
  41.6 0.2 collective-permute-done.8.refs_1_
  41.8 0.6 %collective-permute-done.9.refs_2_ = f32[40,128]{1,0:T(8,128)S(1)} collective-permute-done((f32[40,128]{1,0:T(8,128)S(1)}, f32[40,128]{1,0:T(8,128)S(1)}, u32[]{:S(2)}, u32[]{:S(2)}) %collective-permute-start.9) | collective-permute-done | bytes 20512 | tf_op jit(solution)/shard_map/ppermute | solution.py:519
  42.4 0.6 %place_outputs.1 = (bf16[2,4,16,128]{3,2,1,0:T(8,128)(2,1)}, bf16[2,512]{1,0:T(2,128)(2,1)}) custom-call(f32[40,128]{1,0:T(8,128)S(1)} %get-tuple-element.38.refs_0_, f32[40,128]{1,0:T(8,128)S(1)} %collective-permute-done.8.refs_1_, f32[40,128]{1,0:T(8,128)S(1)} %collective-permute-done.9.refs_2_, f32[40,128]{1,0:T(8,128)S(1)} %collective-permute-done.10.refs_3_), custom_call_target="tpu_custom_call" | custom-call | tf_op jit(solution)/shard_map/place_outputs/pallas_call | solution.py:492
  (19 shorter events, 0.0 us)
Async XLA Ops:
  8.7 12.6 %collective-permute-start = (f32[1,256,128]{2,1,0:T(8,128)S(1)}, f32[1,256,128]{2,1,0:T(8,128)S(1)}, u32[]{:S(2)}, u32[]{:S(2)}) collective-permute-start(f32[1,256,128]{2,1,0:T(8,128)S(1)} %get-tuple-element.23), channel_id=1, source_target_pairs={{0,2},{2,0},{4,6},{6,4},{8,10},{10,8},{12,14},{14,12},{1,3},{3,1},... | collective-permute-start | bytes 393224 | tf_op jit(solution)/shard_map/ppermute | solution.py:519
  11.8 10.3 %collective-permute-start.1 = (f32[1,256,128]{2,1,0:T(8,128)S(1)}, f32[1,256,128]{2,1,0:T(8,128)S(1)}, u32[]{:S(2)}, u32[]{:S(2)}) collective-permute-start(f32[1,256,128]{2,1,0:T(8,128)S(1)} %get-tuple-element.24), channel_id=1, source_target_pairs={{0,4},{2,6},{4,0},{6,2},{8,12},{10,14},{12,8},{14,10},{1,5},{3,7},... | collective-permute-start | bytes 393224 | tf_op jit(solution)/shard_map/ppermute | solution.py:519
  13.4 8.8 %collective-permute-start.2 = (f32[1,256,128]{2,1,0:T(8,128)S(1)}, f32[1,256,128]{2,1,0:T(8,128)S(1)}, u32[]{:S(2)}, u32[]{:S(2)}) collective-permute-start(f32[1,256,128]{2,1,0:T(8,128)S(1)} %get-tuple-element.25), channel_id=1, source_target_pairs={{0,6},{2,4},{4,2},{6,0},{8,14},{10,12},{12,10},{14,8},{1,7},{3,5},... | collective-permute-start | bytes 393224 | tf_op jit(solution)/shard_map/ppermute | solution.py:519
  13.4 7.9 %copy-start = (bf16[2048,512]{1,0:T(8,128)(2,1)S(1)}, bf16[2048,512]{1,0:T(8,128)(2,1)}, u32[]{:S(2)}) copy-start(bf16[2048,512]{1,0:T(8,128)(2,1)} %refs_2_.3) | copy-start | bytes 6291460
  13.4 7.9 %copy-start.1 = (bf16[2048,8]{0,1:T(8,128)(2,1)S(1)}, bf16[2048,8]{0,1:T(8,128)(2,1)}, u32[]{:S(2)}) copy-start(bf16[2048,8]{0,1:T(8,128)(2,1)} %param.16) | copy-start | bytes 98308
  13.4 7.9 %copy-start.2 = (bf16[2048,8]{0,1:T(8,128)(2,1)S(1)}, bf16[2048,8]{0,1:T(8,128)(2,1)}, u32[]{:S(2)}) copy-start(bf16[2048,8]{0,1:T(8,128)(2,1)} %param.17) | copy-start | bytes 98308
  13.4 7.9 %copy-start.3 = (bf16[2,2048]{1,0:T(2,128)(2,1)S(1)}, bf16[2,2048]{1,0:T(2,128)(2,1)}, u32[]{:S(2)}) copy-start(bf16[2,2048]{1,0:T(2,128)(2,1)} %refs_0_.3) | copy-start | bytes 24580
  13.4 7.9 %copy-start.4 = (f32[4]{0:T(128)S(1)}, f32[4]{0:T(128)}, u32[]{:S(2)}) copy-start(f32[4]{0:T(128)} %param.18) | copy-start | bytes 52
  13.4 7.9 %copy-start.5 = (f32[4]{0:T(128)S(1)}, f32[4]{0:T(128)}, u32[]{:S(2)}) copy-start(f32[4]{0:T(128)} %param.19) | copy-start | bytes 52
  17.7 5.9 %collective-permute-start.3 = (f32[1,256,128]{2,1,0:T(8,128)S(1)}, f32[1,256,128]{2,1,0:T(8,128)S(1)}, u32[]{:S(2)}, u32[]{:S(2)}) collective-permute-start(f32[1,256,128]{2,1,0:T(8,128)S(1)} %get-tuple-element.31), channel_id=1, source_target_pairs={{0,2},{2,0},{4,6},{6,4},{8,10},{10,8},{12,14},{14,12},{1,3},{3,1},... | collective-permute-start | bytes 393224 | tf_op jit(solution)/shard_map/ppermute | solution.py:519
  19.7 5.5 %collective-permute-start.4 = (f32[1,256,128]{2,1,0:T(8,128)S(1)}, f32[1,256,128]{2,1,0:T(8,128)S(1)}, u32[]{:S(2)}, u32[]{:S(2)}) collective-permute-start(f32[1,256,128]{2,1,0:T(8,128)S(1)} %get-tuple-element.32), channel_id=1, source_target_pairs={{0,4},{2,6},{4,0},{6,2},{8,12},{10,14},{12,8},{14,10},{1,5},{3,7},... | collective-permute-start | bytes 393224 | tf_op jit(solution)/shard_map/ppermute | solution.py:519
  21.3 15.3 %copy-start.6 = (f32[128]{0:T(128)S(1)}, f32[128]{0:T(128)}, u32[]{:S(2)}) copy-start(f32[128]{0:T(128)} %param.23) | copy-start | bytes 1540
  21.3 5.9 %collective-permute-start.5 = (f32[1,256,128]{2,1,0:T(8,128)S(1)}, f32[1,256,128]{2,1,0:T(8,128)S(1)}, u32[]{:S(2)}, u32[]{:S(2)}) collective-permute-start(f32[1,256,128]{2,1,0:T(8,128)S(1)} %get-tuple-element.33), channel_id=1, source_target_pairs={{0,6},{2,4},{4,2},{6,0},{8,14},{10,12},{12,10},{14,8},{1,7},{3,5},... | collective-permute-start | bytes 393224 | tf_op jit(solution)/shard_map/ppermute | solution.py:519
  27.8 8.7 %collective-permute-start.7 = (f32[136,128]{1,0:T(8,128)S(1)}, f32[136,128]{1,0:T(8,128)S(1)}, u32[]{:S(2)}, u32[]{:S(2)}) collective-permute-start(f32[136,128]{1,0:T(8,128)S(1)} %get-tuple-element.37), channel_id=1, source_target_pairs={{0,8},{2,10},{4,12},{6,14},{8,0},{10,2},{12,4},{14,6},{1,9},{3,11}... | collective-permute-start | bytes 208904 | tf_op jit(solution)/shard_map/ppermute | solution.py:519
  30.7 5.9 %collective-permute-start.6 = (f32[128,128]{1,0:T(8,128)S(1)}, f32[128,128]{1,0:T(8,128)S(1)}, u32[]{:S(2)}, u32[]{:S(2)}) collective-permute-start(f32[128,128]{1,0:T(8,128)S(1)} %get-tuple-element.36), channel_id=1, source_target_pairs={{0,8},{2,10},{4,12},{6,14},{8,0},{10,2},{12,4},{14,6},{1,9},{3,11}... | collective-permute-start | bytes 196616 | tf_op jit(solution)/shard_map/ppermute | solution.py:519
  36.9 4.7 %collective-permute-start.10 = (f32[40,128]{1,0:T(8,128)S(1)}, f32[40,128]{1,0:T(8,128)S(1)}, u32[]{:S(2)}, u32[]{:S(2)}) collective-permute-start(f32[40,128]{1,0:T(8,128)S(1)} %get-tuple-element.41), channel_id=1, source_target_pairs={{0,6},{2,4},{4,2},{6,0},{8,14},{10,12},{12,10},{14,8},{1,7},{3,5},... | collective-permute-start | bytes 61448 | tf_op jit(solution)/shard_map/ppermute | solution.py:519
  37.9 3.9 %collective-permute-start.8 = (f32[40,128]{1,0:T(8,128)S(1)}, f32[40,128]{1,0:T(8,128)S(1)}, u32[]{:S(2)}, u32[]{:S(2)}) collective-permute-start(f32[40,128]{1,0:T(8,128)S(1)} %get-tuple-element.39), channel_id=1, source_target_pairs={{0,2},{2,0},{4,6},{6,4},{8,10},{10,8},{12,14},{14,12},{1,3},{3,1},... | collective-permute-start | bytes 61448 | tf_op jit(solution)/shard_map/ppermute | solution.py:519
  38.6 3.8 %collective-permute-start.9 = (f32[40,128]{1,0:T(8,128)S(1)}, f32[40,128]{1,0:T(8,128)S(1)}, u32[]{:S(2)}, u32[]{:S(2)}) collective-permute-start(f32[40,128]{1,0:T(8,128)S(1)} %get-tuple-element.40), channel_id=1, source_target_pairs={{0,4},{2,6},{4,0},{6,2},{8,12},{10,14},{12,8},{14,10},{1,5},{3,7},... | collective-permute-start | bytes 61448 | tf_op jit(solution)/shard_map/ppermute | solution.py:519

commit v3 on v2

--- a/solution.py
+++ b/solution.py
@@ -88,20 +88,16 @@
 
 
 def local_maps_kernel(*refs, heads, own_heads, first, bits):
-    targets = 2**bits
     if first:
         x_hbm, wk_hbm, wv_hbm = refs[:3]
-        small_hbm = refs[3:9]
-        table_ref, x_s, w_s = refs[9:12]
-        rest = refs[12:]
+        small_hbm, (table_ref, x_s, w_s), rest = refs[3:9], refs[9:12], refs[12:]
     else:
-        x_s, w_s, table_ref = refs[:3]
-        rest = refs[3:]
-    outs, rest = rest[:targets], rest[targets:]
-    k_s, v_s, lower_s, inverse_s, half_s, mask_s, map_s = rest[:7]
-    small_s, sems = rest[7:-1], rest[-1]
+        (x_s, w_s, table_ref), rest = refs[:3], refs[3:]
+    outs, rest = rest[: 2**bits], rest[2**bits :]
+    source_s, map_s = rest[:2]
+    small_s, sems = rest[2:-1], rest[-1]
     seqs, span, width = x_s.shape
-    dim = k_s.shape[-1]
+    dim = source_s.shape[-1] // 2
     count = seqs * span
     chunks = count // CHUNK
     group = len(own_heads)
@@ -109,8 +105,8 @@
 
     if first:
         copies = [pltpu.make_async_copy(x_hbm.at[s], x_s.at[s], sems.at[s]) for s in range(seqs)]
-        for i, (source, target) in enumerate(zip(small_hbm, small_s)):
-            copies.append(pltpu.make_async_copy(source, target, sems.at[seqs + i]))
+        for i, (origin, target) in enumerate(zip(small_hbm, small_s)):
+            copies.append(pltpu.make_async_copy(origin, target, sems.at[seqs + i]))
         base = len(copies)
         for h in range(heads):
             for i, w_hbm in enumerate((wk_hbm, wv_hbm)):
@@ -121,112 +117,127 @@
                         sems.at[base + 2 * h + i],
                     )
                 )
-        for copy in copies:
+        own_copies = copies[base : base + 2 * group]
+        other_copies = copies[base + 2 * group :]
+        for copy in copies[:base] + own_copies:
             copy.start()
 
     row = lax.broadcasted_iota(jnp.int32, (CHUNK, CHUNK), 0)
     col = lax.broadcasted_iota(jnp.int32, (CHUNK, CHUNK), 1)
-    strict = row > col
     eye = jnp.where(row == col, 1.0, 0.0)
+    upper = jnp.where(row <= col, 1.0, 0.0)
 
     def level(m):
         return (row // (2 * m) == col // (2 * m)) & (row // m != col // m)
 
-    for i, m in enumerate(steps):
-        mask_s[i] = jnp.where(level(m), 1.0, 0.0).astype(BF16)
-    mask_s[len(steps)] = jnp.where(strict, 1.0, 0.0).astype(BF16)
+    masks = [jnp.where(level(m), 1.0, 0.0).astype(BF16) for m in steps]
+    strict = jnp.where(row > col, 1.0, 0.0).astype(BF16)
+    eye_short = eye.astype(BF16)
 
     if first:
         for copy in copies[:base]:
             copy.wait()
-    flat = x_s[...].reshape(count, width)
-    if first:
+        for copy in other_copies:
+            copy.start()
         wd, ws, speeds, ceilings = (ref[...] for ref in small_s[:4])
         mult, spike = (
             jnp.concatenate([ref[s] for s in range(seqs)], axis=1) for ref in small_s[4:]
         )
         table_ref[...] = gate_tables(
-            flat, wd, ws, speeds, ceilings, mult, spike, heads, jnp.where(row <= col, 1.0, 0.0)
+            x_s[...].reshape(count, width), wd, ws, speeds, ceilings, mult, spike, heads, upper
         )
-    columns = table_ref[...].T
-
-    def at(c, g, which):
-        return (2 * c + which) * heads + own_heads[g]
-
-    def column(c, g, which):
-        return jnp.broadcast_to(columns[:, at(c, g, which) : at(c, g, which) + 1], (CHUNK, CHUNK))
-
-    pieces = [(g, c) for g in range(group) for c in range(chunks)]
-
-    for g, h in enumerate(own_heads):
-        if first:
-            copies[base + 2 * h].wait()
-            copies[base + 2 * h + 1].wait()
-        raw = dot(flat, w_s[h]).astype(BF16).astype(F32)
-        k_s[g] = unit(silu(raw[:, :dim]))
-        v_s[g] = silu(raw[:, dim:])
-
-    def rows_of(c):
-        return slice(c * CHUNK, (c + 1) * CHUNK)
-
-    for n, (g, c) in enumerate(pieces):
-        short = k_s[g, rows_of(c)].astype(BF16)
-        gram = dot_nt(short, short)
-        place = at(c, g, 1)
-        spread = jnp.exp(jnp.minimum(column(c, g, 1) - table_ref[place : place + 1, :], 0.0))
-        lower = jnp.where(strict, gram * column(c, g, 0) * spread, 0.0)
-        lower_s[n] = lower.astype(BF16)
-        inverse_s[n] = (eye - jnp.where(level(1), lower, 0.0)).astype(BF16)
+        for copy in own_copies:
+            copy.wait()
+    table = table_ref[...]
+    columns = table.T
+
+    def at(c, h, which):
+        return (2 * c + which) * heads + h
+
+    def column(c, h, which):
+        return jnp.broadcast_to(columns[:, at(c, h, which) : at(c, h, which) + 1], (CHUNK, CHUNK))
+
+    def project(h):
+        return dot(x_s[...].reshape(count, width), w_s[h])
+
+    pieces = range(group * chunks)
+    lasts, lowers, inverses, fadeds = [], [], [], []
+
+    def prepare(g, raw):
+        h = own_heads[g]
+        raw = raw.astype(BF16).astype(F32)
+        keys_all = unit(silu(raw[:, :dim]))
+        values_all = silu(raw[:, dim:])
+        for c in range(chunks):
+            n = g * chunks + c
+            keys = keys_all[c * CHUNK : (c + 1) * CHUNK]
+            values = values_all[c * CHUNK : (c + 1) * CHUNK]
+            strength, total_log = column(c, h, 0), column(c, h, 1)
+            last = total_log[CHUNK - 1 : CHUNK]
+            short = keys.astype(BF16)
+            gram = dot_nt(short, short)
+            place = at(c, h, 1)
+            spread = jnp.exp(jnp.minimum(total_log - table[place : place + 1], 0.0))
+            lower = (gram * strength * spread).astype(BF16) * strict
+            lowers.append(lower)
+            inverses.append(eye_short - lower * masks[0])
+            source_s[n, :, :dim] = keys * (strength * jnp.exp(total_log))
+            source_s[n, :, dim:] = values * strength
+            fadeds.append((keys * jnp.exp(last - total_log)).astype(BF16))
+            lasts.append(jnp.exp(last))
+
+    raws = [project(h) for h in own_heads]
+    for g in range(group):
+        prepare(g, raws[g])
 
     for i, m in list(enumerate(steps))[1:]:
+        if m < 16:
+            products = [dot(inverses[n], lowers[n] * masks[i]).astype(BF16) for n in pieces]
+            inverses = [
+                inverses[n] - dot(products[n], inverses[n]).astype(BF16) for n in pieces
+            ]
+            continue
         odd = [slice(o, o + m) for o in range(m, CHUNK, 2 * m)]
-        if m < 16:
-            for n in range(len(pieces)):
-                half_s[n] = dot(inverse_s[n], lower_s[n] * mask_s[i]).astype(BF16)
-            for n in range(len(pieces)):
-                inverse_s[n] = inverse_s[n] - dot(half_s[n], inverse_s[n]).astype(BF16)
-        else:
-            for n in range(len(pieces)):
-                picked = jnp.concatenate([inverse_s[n, o] for o in odd], axis=0)
-                half_s[n, : CHUNK // 2] = dot(picked, lower_s[n] * mask_s[i]).astype(BF16)
-            for n in range(len(pieces)):
-                change = dot(half_s[n, : CHUNK // 2], inverse_s[n]).astype(BF16)
-                for j, o in enumerate(odd):
-                    inverse_s[n, o] = inverse_s[n, o] - change[j * m : (j + 1) * m]
+        products = []
+        for n in pieces:
+            picked = jnp.concatenate([inverses[n][o] for o in odd], axis=0)
+            products.append(dot(picked, lowers[n] * masks[i]).astype(BF16))
+        for n in pieces:
+            change = dot(products[n], inverses[n]).astype(BF16)
+            parts = []
+            for j, o in enumerate(odd):
+                parts.append(inverses[n][o.start - m : o.start])
+                parts.append(inverses[n][o] - change[j * m : (j + 1) * m])
+            inverses[n] = jnp.concatenate(parts, axis=0)
 
     terms = []
-    for n, (g, c) in enumerate(pieces):
-        keys, values = k_s[g, rows_of(c)], v_s[g, rows_of(c)]
-        strength, total_log = column(c, g, 0), column(c, g, 1)
-        last = total_log[CHUNK - 1 : CHUNK]
-        off = inverse_s[n] * mask_s[len(steps)]
-        source = jnp.concatenate([keys * (strength * jnp.exp(total_log)), values * strength], axis=1)
+    for n in pieces:
+        off = inverses[n] - eye_short
+        source = source_s[n]
         solved = source + dot(off, source.astype(BF16))
-        faded = (keys * jnp.exp(last - total_log)).astype(BF16)
-        change = dot_tn(faded, solved.astype(BF16))
-        terms.append((change[:, :dim], change[:, dim:], jnp.exp(last)))
+        terms.append(dot_tn(fadeds[n], solved.astype(BF16)))
 
     per = chunks // seqs
+    place = lax.axis_index("sp")
+    states = seqs * group
     for g in range(group):
         for s in range(seqs):
-            mine = terms[g * chunks + s * per : g * chunks + (s + 1) * per]
-            eraser, target, decay = mine[0]
-            held_a, held_b = decay * eye - eraser, target
-            for eraser, target, decay in mine[1:]:
+            n = g * chunks + s * per
+            held_a, held_b = lasts[n] * eye - terms[n][:, :dim], terms[n][:, dim:]
+            for n in range(n + 1, n + per):
                 change = dot(
-                    eraser.astype(BF16), jnp.concatenate([held_a, held_b], axis=1).astype(BF16)
+                    terms[n][:, :dim].astype(BF16),
+                    jnp.concatenate([held_a, held_b], axis=1).astype(BF16),
                 )
-                held_a = decay * held_a - change[:, :dim]
-                held_b = decay * held_b - change[:, dim:] + target
+                held_a = lasts[n] * held_a - change[:, :dim]
+                held_b = lasts[n] * held_b - change[:, dim:] + terms[n][:, dim:]
             map_s[s * group + g, :dim, :] = held_a
             map_s[s * group + g, dim:, :] = held_b
-    states = seqs * group >> bits
-    place = lax.axis_index("sp")
     for mask, out in enumerate(outs):
-        for i in range(states):
-            out[i] = map_s[state_index(i, place ^ mask, seqs * group, bits)]
+        for i in range(states >> bits):
+            out[i] = map_s[state_index(i, place ^ mask, states, bits)]
     if first:
-        for copy in copies[base + 2 * len(own_heads) :]:
+        for copy in other_copies:
             copy.wait()
 
 
@@ -234,17 +245,12 @@
     seqs, span, width = x.shape
     count = seqs * span
     group = len(own_heads)
+    states = seqs * group
     pieces = group * count // CHUNK
-    square = (CHUNK, CHUNK)
-    results = [pltpu.VMEM((seqs * group >> bits, 2 * dim, dim), F32)] * 2**bits
+    results = [pltpu.VMEM((states >> bits, 2 * dim, dim), F32)] * 2**bits
     scratch = [
-        pltpu.VMEM((group, count, dim), F32),
-        pltpu.VMEM((group, count, dim), F32),
-        pltpu.VMEM((pieces,) + square, BF16),
-        pltpu.VMEM((pieces,) + square, BF16),
-        pltpu.VMEM((pieces,) + square, BF16),
-        pltpu.VMEM((CHUNK.bit_length(),) + square, BF16),
-        pltpu.VMEM((seqs * group, 2 * dim, dim), F32),
+        pltpu.VMEM((pieces, CHUNK, 2 * dim), F32),
+        pltpu.VMEM((states, 2 * dim, dim), F32),
     ]
     first = table is None
     if first:
@@ -540,7 +546,10 @@
         results = local_maps(x, w, small, heads, own_heads, dim, bits, table)
         if table is None:
             table, x, w, *results = results
-        flows.append([part if m == 0 else exchange(part, m) for m, part in enumerate(results)])
+        flow = [results[0]] + [None] * (len(results) - 1)
+        for m in range(1, len(results)):
+            flow[m] = exchange(results[m], m)
+        flows.append(flow)
     token = new_token(upcoming_element_vector, w, lookup_weights, small, groups, bits, dim)
     low, span = 0, bits
     while low + span < top:

time: 43.2 us -> 41.3 us (0.956)
  Pallas kernels: 15.3 us -> 13.4 us
    pallas_call x2, Pallas kernels: 12.4 us -> 10.5 us  [local_maps(): pl.pallas_call(lambda *refs: local_maps_kernel(*refs, heads=heads, own_he...]
where the time goes in v3:
time: 41.3 us; the launch traced here: 41.2 us
  starting transfers between devices  14.7 us (36%)
  Pallas kernels  13.4 us (32%)
  waiting for transfers between devices  12.3 us (30%)
  between operations  0.74 us (2%)
    ppermute x11, starting transfers between devices, exchange(): got = lax.ppermute(values, 'sp', [(i, i ^ mask) for i in range(places)])  14.7 us
    ppermute x11, waiting for transfers between devices, exchange(): got = lax.ppermute(values, 'sp', [(i, i ^ mask) for i in range(places)])  12.3 us
    pallas_call x2, Pallas kernels, local_maps(): pl.pallas_call(lambda *refs: local_maps_kernel(*refs, heads=heads, own_he...  10.5 us
    pallas_call x2, Pallas kernels, pack(): pl.pallas_call(lambda *refs: pack_kernel(*refs, count=len(parts), earlier...  1.23 us
  transfers between devices with their start and end apart: 11, of which 7 were waited for; matrix products, arithmetic and copies ran while one was open for 0% of the time, Pallas kernels for 13%

profile of v3, /device:TPU:0, one launch (start us, length us, event | category | flops | bytes accessed | tf_op | source)
XLA Modules:
  0.0 41.2 jit_solution(8461929654633359542)
XLA Ops:
  0.6 6.5 %local_maps.2 = (f32[32,128]{1,0:T(8,128)S(1)}, bf16[2,256,2048]{2,1,0:T(8,128)(2,1)S(1)}, bf16[4,2048,256]{2,1,0:T(8,128)(2,1)S(1)}, f32[1,256,128]{2,1,0:T(8,1...) custom-call(bf16[2,256,2048]{2,1,0:T(8,128)(2,1)} %refs_0_.2, ...), custom_call_target="tpu_custom_call" | custom-call | tf_op jit(solution)/shard_map/local_maps/pallas_call | solution.py:270
  7.2 3.1 %collective-permute-start = (f32[1,256,128]{2,1,0:T(8,128)S(1)}, f32[1,256,128]{2,1,0:T(8,128)S(1)}, u32[]{:S(2)}, u32[]{:S(2)}) collective-permute-start(f32[1,256,128]{2,1,0:T(8,128)S(1)} %get-tuple-element.23), channel_id=1, source_target_pairs={{0,2},{2,0},{4,6},{6,4},{8,10},{10,8},{12,14},{14,12},{1,3},{3,1},... | collective-permute-start | bytes 393224 | tf_op jit(solution)/shard_map/ppermute | solution.py:525
  10.2 1.6 %collective-permute-start.1 = (f32[1,256,128]{2,1,0:T(8,128)S(1)}, f32[1,256,128]{2,1,0:T(8,128)S(1)}, u32[]{:S(2)}, u32[]{:S(2)}) collective-permute-start(f32[1,256,128]{2,1,0:T(8,128)S(1)} %get-tuple-element.24), channel_id=1, source_target_pairs={{0,4},{2,6},{4,0},{6,2},{8,12},{10,14},{12,8},{14,10},{1,5},{3,7},... | collective-permute-start | bytes 393224 | tf_op jit(solution)/shard_map/ppermute | solution.py:525
  11.8 4.0 %local_maps.3 = (f32[1,256,128]{2,1,0:T(8,128)S(1)}, f32[1,256,128]{2,1,0:T(8,128)S(1)}, f32[1,256,128]{2,1,0:T(8,128)S(1)}, f32[1,256,128]{2,1,0:T(8,128)S(1)}) custom-call(bf16[2,256,2048]{2,1,0:T(8,128)(2,1)S(1)} %get-tuple-element.27.refs_0_, bf16[4,2048,256]{2,1,0:T(8,128)(2,1)S(1)} %get-tuple-element.28.refs_1_, f32[32,128]{1,0:T(8,128)S(1)} %get-tuple-element.29.refs_2_), custom_call_target="tpu_custom_call" | custom-call | tf_op jit(solution)/shard_map/local_maps/pallas_call | solution.py:270
  15.8 2.0 %collective-permute-start.3 = (f32[1,256,128]{2,1,0:T(8,128)S(1)}, f32[1,256,128]{2,1,0:T(8,128)S(1)}, u32[]{:S(2)}, u32[]{:S(2)}) collective-permute-start(f32[1,256,128]{2,1,0:T(8,128)S(1)} %get-tuple-element.31), channel_id=1, source_target_pairs={{0,2},{2,0},{4,6},{6,4},{8,10},{10,8},{12,14},{14,12},{1,3},{3,1},... | collective-permute-start | bytes 393224 | tf_op jit(solution)/shard_map/ppermute | solution.py:525
  17.8 1.6 %collective-permute-start.4 = (f32[1,256,128]{2,1,0:T(8,128)S(1)}, f32[1,256,128]{2,1,0:T(8,128)S(1)}, u32[]{:S(2)}, u32[]{:S(2)}) collective-permute-start(f32[1,256,128]{2,1,0:T(8,128)S(1)} %get-tuple-element.32), channel_id=1, source_target_pairs={{0,4},{2,6},{4,0},{6,2},{8,12},{10,14},{12,8},{14,10},{1,5},{3,7},... | collective-permute-start | bytes 393224 | tf_op jit(solution)/shard_map/ppermute | solution.py:525
  19.4 0.0 collective-permute-start.5
  19.4 0.8 %new_token.1.refs_5_.refs_4_ = f32[2,8,128]{2,1,0:T(8,128)S(1)} custom-call(bf16[2,2048]{1,0:T(2,128)(2,1)S(1)} %copy-done.3, bf16[4,2048,256]{2,1,0:T(8,128)(2,1)S(1)} %get-tuple-element.28.refs_1_, bf16[2048,512]{1,0:T(8,128)(2,1)S(1)} %copy-done, bf16[8,2048]{1,0:T(8,128)(2,1)S(1)} %bitcast.8, bf16[8,2048]{1,0:T(8,128)(2,1)S(1)} %bitcast.10, ...), custom_call_target="tpu_custom_call" | custom-call | tf_op jit(solution)/shard_map/new_token/pallas_call | solution.py:329
  20.2 0.5 %pack.2 = (f32[128,128]{1,0:T(8,128)S(1)}, f32[128,128]{1,0:T(8,128)S(1)}, f32[1,256,128]{2,1,0:T(8,128)S(1)}) custom-call(f32[1,256,128]{2,1,0:T(8,128)S(1)} %get-tuple-element.22.refs_0_, f32[1,256,128]{2,1,0:T(8,128)S(1)} %collective-permute-done.refs_1_, f32[1,256,128]{2,1,0:T(8,128)S(1)} %collective-permute-done.1.refs_2_, ...), custom_call_target="tpu_custom_call" | custom-call | tf_op jit(solution)/shard_map/pack/pallas_call | solution.py:415
  20.7 0.9 %collective-permute-done.3.refs_1_ = f32[1,256,128]{2,1,0:T(8,128)S(1)} collective-permute-done((f32[1,256,128]{2,1,0:T(8,128)S(1)}, f32[1,256,128]{2,1,0:T(8,128)S(1)}, u32[]{:S(2)}, u32[]{:S(2)}) %collective-permute-start.3) | collective-permute-done | bytes 131104 | tf_op jit(solution)/shard_map/ppermute | solution.py:525
  21.7 1.6 %collective-permute-done.4.refs_2_ = f32[1,256,128]{2,1,0:T(8,128)S(1)} collective-permute-done((f32[1,256,128]{2,1,0:T(8,128)S(1)}, f32[1,256,128]{2,1,0:T(8,128)S(1)}, u32[]{:S(2)}, u32[]{:S(2)}) %collective-permute-start.4) | collective-permute-done | bytes 131104 | tf_op jit(solution)/shard_map/ppermute | solution.py:525
  23.3 1.9 %collective-permute-done.5.refs_3_ = f32[1,256,128]{2,1,0:T(8,128)S(1)} collective-permute-done((f32[1,256,128]{2,1,0:T(8,128)S(1)}, f32[1,256,128]{2,1,0:T(8,128)S(1)}, u32[]{:S(2)}, u32[]{:S(2)}) %collective-permute-start.5) | collective-permute-done | bytes 131104 | tf_op jit(solution)/shard_map/ppermute | solution.py:525
  25.2 0.7 %pack.3 = (f32[136,128]{1,0:T(8,128)S(1)}, f32[136,128]{1,0:T(8,128)S(1)}) custom-call(f32[1,256,128]{2,1,0:T(8,128)S(1)} %get-tuple-element.30.refs_0_, f32[1,256,128]{2,1,0:T(8,128)S(1)} %collective-permute-done.3.refs_1_, f32[1,256,128]{2,1,0:T(8,128)S(1)} %collective-permute-done.4.refs_2_, f32[1,256,128]{2,1,0:T(8,128)S(1)} %collective-permute-done.5.refs_3_, ...), custom_call_target="tpu_custom_call" | custom-call | tf_op jit(solution)/shard_map/pack/pallas_call | solution.py:415
  25.9 2.9 %collective-permute-start.7 = (f32[136,128]{1,0:T(8,128)S(1)}, f32[136,128]{1,0:T(8,128)S(1)}, u32[]{:S(2)}, u32[]{:S(2)}) collective-permute-start(f32[136,128]{1,0:T(8,128)S(1)} %get-tuple-element.37), channel_id=1, source_target_pairs={{0,8},{2,10},{4,12},{6,14},{8,0},{10,2},{12,4},{14,6},{1,9},{3,11}... | collective-permute-start | bytes 208904 | tf_op jit(solution)/shard_map/ppermute | solution.py:525
  28.8 0.1 collective-permute-start.6
  28.8 5.8 %collective-permute-done.6.refs_2_ = f32[128,128]{1,0:T(8,128)S(1)} collective-permute-done((f32[128,128]{1,0:T(8,128)S(1)}, f32[128,128]{1,0:T(8,128)S(1)}, u32[]{:S(2)}, u32[]{:S(2)}) %collective-permute-start.6) | collective-permute-done | bytes 65568 | tf_op jit(solution)/shard_map/ppermute | solution.py:525
  34.7 0.3 finish.1
  35.0 1.0 %collective-permute-start.10 = (f32[40,128]{1,0:T(8,128)S(1)}, f32[40,128]{1,0:T(8,128)S(1)}, u32[]{:S(2)}, u32[]{:S(2)}) collective-permute-start(f32[40,128]{1,0:T(8,128)S(1)} %get-tuple-element.41), channel_id=1, source_target_pairs={{0,6},{2,4},{4,2},{6,0},{8,14},{10,12},{12,10},{14,8},{1,7},{3,5},... | collective-permute-start | bytes 61448 | tf_op jit(solution)/shard_map/ppermute | solution.py:525
  36.0 0.7 %collective-permute-start.8 = (f32[40,128]{1,0:T(8,128)S(1)}, f32[40,128]{1,0:T(8,128)S(1)}, u32[]{:S(2)}, u32[]{:S(2)}) collective-permute-start(f32[40,128]{1,0:T(8,128)S(1)} %get-tuple-element.39), channel_id=1, source_target_pairs={{0,2},{2,0},{4,6},{6,4},{8,10},{10,8},{12,14},{14,12},{1,3},{3,1},... | collective-permute-start | bytes 61448 | tf_op jit(solution)/shard_map/ppermute | solution.py:525
  36.7 1.8 %collective-permute-start.9 = (f32[40,128]{1,0:T(8,128)S(1)}, f32[40,128]{1,0:T(8,128)S(1)}, u32[]{:S(2)}, u32[]{:S(2)}) collective-permute-start(f32[40,128]{1,0:T(8,128)S(1)} %get-tuple-element.40), channel_id=1, source_target_pairs={{0,4},{2,6},{4,0},{6,2},{8,12},{10,14},{12,8},{14,10},{1,5},{3,7},... | collective-permute-start | bytes 61448 | tf_op jit(solution)/shard_map/ppermute | solution.py:525
  38.5 1.2 %collective-permute-done.10.refs_3_ = f32[40,128]{1,0:T(8,128)S(1)} collective-permute-done((f32[40,128]{1,0:T(8,128)S(1)}, f32[40,128]{1,0:T(8,128)S(1)}, u32[]{:S(2)}, u32[]{:S(2)}) %collective-permute-start.10) | collective-permute-done | bytes 20512 | tf_op jit(solution)/shard_map/ppermute | solution.py:525
  39.7 0.2 collective-permute-done.8.refs_1_
  39.9 0.6 %collective-permute-done.9.refs_2_ = f32[40,128]{1,0:T(8,128)S(1)} collective-permute-done((f32[40,128]{1,0:T(8,128)S(1)}, f32[40,128]{1,0:T(8,128)S(1)}, u32[]{:S(2)}, u32[]{:S(2)}) %collective-permute-start.9) | collective-permute-done | bytes 20512 | tf_op jit(solution)/shard_map/ppermute | solution.py:525
  40.5 0.6 %place_outputs.1 = (bf16[2,4,16,128]{3,2,1,0:T(8,128)(2,1)}, bf16[2,512]{1,0:T(2,128)(2,1)}) custom-call(f32[40,128]{1,0:T(8,128)S(1)} %get-tuple-element.38.refs_0_, f32[40,128]{1,0:T(8,128)S(1)} %collective-permute-done.8.refs_1_, f32[40,128]{1,0:T(8,128)S(1)} %collective-permute-done.9.refs_2_, f32[40,128]{1,0:T(8,128)S(1)} %collective-permute-done.10.refs_3_), custom_call_target="tpu_custom_call" | custom-call | tf_op jit(solution)/shard_map/place_outputs/pallas_call | solution.py:498
  (19 shorter events, 0.0 us)
Async XLA Ops:
  7.2 12.2 %collective-permute-start = (f32[1,256,128]{2,1,0:T(8,128)S(1)}, f32[1,256,128]{2,1,0:T(8,128)S(1)}, u32[]{:S(2)}, u32[]{:S(2)}) collective-permute-start(f32[1,256,128]{2,1,0:T(8,128)S(1)} %get-tuple-element.23), channel_id=1, source_target_pairs={{0,2},{2,0},{4,6},{6,4},{8,10},{10,8},{12,14},{14,12},{1,3},{3,1},... | collective-permute-start | bytes 393224 | tf_op jit(solution)/shard_map/ppermute | solution.py:525
  10.2 10.0 %collective-permute-start.1 = (f32[1,256,128]{2,1,0:T(8,128)S(1)}, f32[1,256,128]{2,1,0:T(8,128)S(1)}, u32[]{:S(2)}, u32[]{:S(2)}) collective-permute-start(f32[1,256,128]{2,1,0:T(8,128)S(1)} %get-tuple-element.24), channel_id=1, source_target_pairs={{0,4},{2,6},{4,0},{6,2},{8,12},{10,14},{12,8},{14,10},{1,5},{3,7},... | collective-permute-start | bytes 393224 | tf_op jit(solution)/shard_map/ppermute | solution.py:525
  11.8 8.4 %collective-permute-start.2 = (f32[1,256,128]{2,1,0:T(8,128)S(1)}, f32[1,256,128]{2,1,0:T(8,128)S(1)}, u32[]{:S(2)}, u32[]{:S(2)}) collective-permute-start(f32[1,256,128]{2,1,0:T(8,128)S(1)} %get-tuple-element.25), channel_id=1, source_target_pairs={{0,6},{2,4},{4,2},{6,0},{8,14},{10,12},{12,10},{14,8},{1,7},{3,5},... | collective-permute-start | bytes 393224 | tf_op jit(solution)/shard_map/ppermute | solution.py:525
  11.8 7.6 %copy-start = (bf16[2048,512]{1,0:T(8,128)(2,1)S(1)}, bf16[2048,512]{1,0:T(8,128)(2,1)}, u32[]{:S(2)}) copy-start(bf16[2048,512]{1,0:T(8,128)(2,1)} %refs_2_.3) | copy-start | bytes 6291460
  11.8 7.6 %copy-start.1 = (bf16[2048,8]{0,1:T(8,128)(2,1)S(1)}, bf16[2048,8]{0,1:T(8,128)(2,1)}, u32[]{:S(2)}) copy-start(bf16[2048,8]{0,1:T(8,128)(2,1)} %param.16) | copy-start | bytes 98308
  11.8 7.6 %copy-start.2 = (bf16[2048,8]{0,1:T(8,128)(2,1)S(1)}, bf16[2048,8]{0,1:T(8,128)(2,1)}, u32[]{:S(2)}) copy-start(bf16[2048,8]{0,1:T(8,128)(2,1)} %param.17) | copy-start | bytes 98308
  11.8 7.6 %copy-start.3 = (bf16[2,2048]{1,0:T(2,128)(2,1)S(1)}, bf16[2,2048]{1,0:T(2,128)(2,1)}, u32[]{:S(2)}) copy-start(bf16[2,2048]{1,0:T(2,128)(2,1)} %refs_0_.3) | copy-start | bytes 24580
  11.8 7.6 %copy-start.4 = (f32[4]{0:T(128)S(1)}, f32[4]{0:T(128)}, u32[]{:S(2)}) copy-start(f32[4]{0:T(128)} %param.18) | copy-start | bytes 52
  11.8 7.6 %copy-start.5 = (f32[4]{0:T(128)S(1)}, f32[4]{0:T(128)}, u32[]{:S(2)}) copy-start(f32[4]{0:T(128)} %param.19) | copy-start | bytes 52
  15.8 5.9 %collective-permute-start.3 = (f32[1,256,128]{2,1,0:T(8,128)S(1)}, f32[1,256,128]{2,1,0:T(8,128)S(1)}, u32[]{:S(2)}, u32[]{:S(2)}) collective-permute-start(f32[1,256,128]{2,1,0:T(8,128)S(1)} %get-tuple-element.31), channel_id=1, source_target_pairs={{0,2},{2,0},{4,6},{6,4},{8,10},{10,8},{12,14},{14,12},{1,3},{3,1},... | collective-permute-start | bytes 393224 | tf_op jit(solution)/shard_map/ppermute | solution.py:525
  17.8 5.5 %collective-permute-start.4 = (f32[1,256,128]{2,1,0:T(8,128)S(1)}, f32[1,256,128]{2,1,0:T(8,128)S(1)}, u32[]{:S(2)}, u32[]{:S(2)}) collective-permute-start(f32[1,256,128]{2,1,0:T(8,128)S(1)} %get-tuple-element.32), channel_id=1, source_target_pairs={{0,4},{2,6},{4,0},{6,2},{8,12},{10,14},{12,8},{14,10},{1,5},{3,7},... | collective-permute-start | bytes 393224 | tf_op jit(solution)/shard_map/ppermute | solution.py:525
  19.4 15.3 %copy-start.6 = (f32[128]{0:T(128)S(1)}, f32[128]{0:T(128)}, u32[]{:S(2)}) copy-start(f32[128]{0:T(128)} %param.23) | copy-start | bytes 1540
  19.4 5.9 %collective-permute-start.5 = (f32[1,256,128]{2,1,0:T(8,128)S(1)}, f32[1,256,128]{2,1,0:T(8,128)S(1)}, u32[]{:S(2)}, u32[]{:S(2)}) collective-permute-start(f32[1,256,128]{2,1,0:T(8,128)S(1)} %get-tuple-element.33), channel_id=1, source_target_pairs={{0,6},{2,4},{4,2},{6,0},{8,14},{10,12},{12,10},{14,8},{1,7},{3,5},... | collective-permute-start | bytes 393224 | tf_op jit(solution)/shard_map/ppermute | solution.py:525
  25.9 8.7 %collective-permute-start.7 = (f32[136,128]{1,0:T(8,128)S(1)}, f32[136,128]{1,0:T(8,128)S(1)}, u32[]{:S(2)}, u32[]{:S(2)}) collective-permute-start(f32[136,128]{1,0:T(8,128)S(1)} %get-tuple-element.37), channel_id=1, source_target_pairs={{0,8},{2,10},{4,12},{6,14},{8,0},{10,2},{12,4},{14,6},{1,9},{3,11}... | collective-permute-start | bytes 208904 | tf_op jit(solution)/shard_map/ppermute | solution.py:525
  28.8 5.9 %collective-permute-start.6 = (f32[128,128]{1,0:T(8,128)S(1)}, f32[128,128]{1,0:T(8,128)S(1)}, u32[]{:S(2)}, u32[]{:S(2)}) collective-permute-start(f32[128,128]{1,0:T(8,128)S(1)} %get-tuple-element.36), channel_id=1, source_target_pairs={{0,8},{2,10},{4,12},{6,14},{8,0},{10,2},{12,4},{14,6},{1,9},{3,11}... | collective-permute-start | bytes 196616 | tf_op jit(solution)/shard_map/ppermute | solution.py:525
  35.0 4.7 %collective-permute-start.10 = (f32[40,128]{1,0:T(8,128)S(1)}, f32[40,128]{1,0:T(8,128)S(1)}, u32[]{:S(2)}, u32[]{:S(2)}) collective-permute-start(f32[40,128]{1,0:T(8,128)S(1)} %get-tuple-element.41), channel_id=1, source_target_pairs={{0,6},{2,4},{4,2},{6,0},{8,14},{10,12},{12,10},{14,8},{1,7},{3,5},... | collective-permute-start | bytes 61448 | tf_op jit(solution)/shard_map/ppermute | solution.py:525
  36.0 3.9 %collective-permute-start.8 = (f32[40,128]{1,0:T(8,128)S(1)}, f32[40,128]{1,0:T(8,128)S(1)}, u32[]{:S(2)}, u32[]{:S(2)}) collective-permute-start(f32[40,128]{1,0:T(8,128)S(1)} %get-tuple-element.39), channel_id=1, source_target_pairs={{0,2},{2,0},{4,6},{6,4},{8,10},{10,8},{12,14},{14,12},{1,3},{3,1},... | collective-permute-start | bytes 61448 | tf_op jit(solution)/shard_map/ppermute | solution.py:525
  36.7 3.8 %collective-permute-start.9 = (f32[40,128]{1,0:T(8,128)S(1)}, f32[40,128]{1,0:T(8,128)S(1)}, u32[]{:S(2)}, u32[]{:S(2)}) collective-permute-start(f32[40,128]{1,0:T(8,128)S(1)} %get-tuple-element.40), channel_id=1, source_target_pairs={{0,4},{2,6},{4,0},{6,2},{8,12},{10,14},{12,8},{14,10},{1,5},{3,7},... | collective-permute-start | bytes 61448 | tf_op jit(solution)/shard_map/ppermute | solution.py:525

commit v4 on v3

--- a/solution.py
+++ b/solution.py
@@ -137,8 +137,6 @@
     if first:
         for copy in copies[:base]:
             copy.wait()
-        for copy in other_copies:
-            copy.start()
         wd, ws, speeds, ceilings = (ref[...] for ref in small_s[:4])
         mult, spike = (
             jnp.concatenate([ref[s] for s in range(seqs)], axis=1) for ref in small_s[4:]
@@ -148,6 +146,8 @@
         )
         for copy in own_copies:
             copy.wait()
+        for copy in other_copies:
+            copy.start()
     table = table_ref[...]
     columns = table.T
 
@@ -157,21 +157,16 @@
     def column(c, h, which):
         return jnp.broadcast_to(columns[:, at(c, h, which) : at(c, h, which) + 1], (CHUNK, CHUNK))
 
-    def project(h):
-        return dot(x_s[...].reshape(count, width), w_s[h])
-
     pieces = range(group * chunks)
     lasts, lowers, inverses, fadeds = [], [], [], []
 
     def prepare(g, raw):
         h = own_heads[g]
-        raw = raw.astype(BF16).astype(F32)
-        keys_all = unit(silu(raw[:, :dim]))
-        values_all = silu(raw[:, dim:])
         for c in range(chunks):
             n = g * chunks + c
-            keys = keys_all[c * CHUNK : (c + 1) * CHUNK]
-            values = values_all[c * CHUNK : (c + 1) * CHUNK]
+            part = raw[c * CHUNK : (c + 1) * CHUNK].astype(BF16).astype(F32)
+            keys = unit(silu(part[:, :dim]))
+            values = silu(part[:, dim:])
             strength, total_log = column(c, h, 0), column(c, h, 1)
             last = total_log[CHUNK - 1 : CHUNK]
             short = keys.astype(BF16)
@@ -186,7 +181,9 @@
             fadeds.append((keys * jnp.exp(last - total_log)).astype(BF16))
             lasts.append(jnp.exp(last))
 
-    raws = [project(h) for h in own_heads]
+    raws = [
+        jnp.concatenate([dot(x_s[s], w_s[h]) for s in range(seqs)], axis=0) for h in own_heads
+    ]
     for g in range(group):
         prepare(g, raws[g])
 

time: 41.3 us -> 41.1 us (level)
  no operation moved by 1% of the time
where the time goes in v4:
time: 41.1 us; the launch traced here: 40.9 us
  starting transfers between devices  14.7 us (36%)
  Pallas kernels  13.2 us (32%)
  waiting for transfers between devices  12.3 us (30%)
  between operations  0.73 us (2%)
    ppermute x11, starting transfers between devices, exchange(): got = lax.ppermute(values, 'sp', [(i, i ^ mask) for i in range(places)])  14.7 us
    ppermute x11, waiting for transfers between devices, exchange(): got = lax.ppermute(values, 'sp', [(i, i ^ mask) for i in range(places)])  12.3 us
    pallas_call x2, Pallas kernels, local_maps(): pl.pallas_call(lambda *refs: local_maps_kernel(*refs, heads=heads, own_he...  10.2 us
    pallas_call x2, Pallas kernels, pack(): pl.pallas_call(lambda *refs: pack_kernel(*refs, count=len(parts), earlier...  1.23 us
  transfers between devices with their start and end apart: 11, of which 7 were waited for; matrix products, arithmetic and copies ran while one was open for 0% of the time, Pallas kernels for 13%

profile of v4, /device:TPU:0, one launch (start us, length us, event | category | flops | bytes accessed | tf_op | source)
XLA Modules:
  0.0 40.9 jit_solution(14422615612617418334)
XLA Ops:
  0.6 6.4 %local_maps.2 = (f32[32,128]{1,0:T(8,128)S(1)}, bf16[2,256,2048]{2,1,0:T(8,128)(2,1)S(1)}, bf16[4,2048,256]{2,1,0:T(8,128)(2,1)S(1)}, f32[1,256,128]{2,1,0:T(8,1...) custom-call(bf16[2,256,2048]{2,1,0:T(8,128)(2,1)} %refs_0_.2, ...), custom_call_target="tpu_custom_call" | custom-call | tf_op jit(solution)/shard_map/local_maps/pallas_call | solution.py:267
  7.0 3.1 %collective-permute-start = (f32[1,256,128]{2,1,0:T(8,128)S(1)}, f32[1,256,128]{2,1,0:T(8,128)S(1)}, u32[]{:S(2)}, u32[]{:S(2)}) collective-permute-start(f32[1,256,128]{2,1,0:T(8,128)S(1)} %get-tuple-element.23), channel_id=1, source_target_pairs={{0,2},{2,0},{4,6},{6,4},{8,10},{10,8},{12,14},{14,12},{1,3},{3,1},... | collective-permute-start | bytes 393224 | tf_op jit(solution)/shard_map/ppermute | solution.py:522
  10.1 1.6 %collective-permute-start.1 = (f32[1,256,128]{2,1,0:T(8,128)S(1)}, f32[1,256,128]{2,1,0:T(8,128)S(1)}, u32[]{:S(2)}, u32[]{:S(2)}) collective-permute-start(f32[1,256,128]{2,1,0:T(8,128)S(1)} %get-tuple-element.24), channel_id=1, source_target_pairs={{0,4},{2,6},{4,0},{6,2},{8,12},{10,14},{12,8},{14,10},{1,5},{3,7},... | collective-permute-start | bytes 393224 | tf_op jit(solution)/shard_map/ppermute | solution.py:522
  11.7 3.8 %local_maps.3 = (f32[1,256,128]{2,1,0:T(8,128)S(1)}, f32[1,256,128]{2,1,0:T(8,128)S(1)}, f32[1,256,128]{2,1,0:T(8,128)S(1)}, f32[1,256,128]{2,1,0:T(8,128)S(1)}) custom-call(bf16[2,256,2048]{2,1,0:T(8,128)(2,1)S(1)} %get-tuple-element.27.refs_0_, bf16[4,2048,256]{2,1,0:T(8,128)(2,1)S(1)} %get-tuple-element.28.refs_1_, f32[32,128]{1,0:T(8,128)S(1)} %get-tuple-element.29.refs_2_), custom_call_target="tpu_custom_call" | custom-call | tf_op jit(solution)/shard_map/local_maps/pallas_call | solution.py:267
  15.6 2.0 %collective-permute-start.3 = (f32[1,256,128]{2,1,0:T(8,128)S(1)}, f32[1,256,128]{2,1,0:T(8,128)S(1)}, u32[]{:S(2)}, u32[]{:S(2)}) collective-permute-start(f32[1,256,128]{2,1,0:T(8,128)S(1)} %get-tuple-element.31), channel_id=1, source_target_pairs={{0,2},{2,0},{4,6},{6,4},{8,10},{10,8},{12,14},{14,12},{1,3},{3,1},... | collective-permute-start | bytes 393224 | tf_op jit(solution)/shard_map/ppermute | solution.py:522
  17.5 1.6 %collective-permute-start.4 = (f32[1,256,128]{2,1,0:T(8,128)S(1)}, f32[1,256,128]{2,1,0:T(8,128)S(1)}, u32[]{:S(2)}, u32[]{:S(2)}) collective-permute-start(f32[1,256,128]{2,1,0:T(8,128)S(1)} %get-tuple-element.32), channel_id=1, source_target_pairs={{0,4},{2,6},{4,0},{6,2},{8,12},{10,14},{12,8},{14,10},{1,5},{3,7},... | collective-permute-start | bytes 393224 | tf_op jit(solution)/shard_map/ppermute | solution.py:522
  19.1 0.0 collective-permute-start.5
  19.2 0.8 %new_token.1.refs_5_.refs_4_ = f32[2,8,128]{2,1,0:T(8,128)S(1)} custom-call(bf16[2,2048]{1,0:T(2,128)(2,1)S(1)} %copy-done.3, bf16[4,2048,256]{2,1,0:T(8,128)(2,1)S(1)} %get-tuple-element.28.refs_1_, bf16[2048,512]{1,0:T(8,128)(2,1)S(1)} %copy-done, bf16[8,2048]{1,0:T(8,128)(2,1)S(1)} %bitcast.8, bf16[8,2048]{1,0:T(8,128)(2,1)S(1)} %bitcast.10, ...), custom_call_target="tpu_custom_call" | custom-call | tf_op jit(solution)/shard_map/new_token/pallas_call | solution.py:326
  19.9 0.5 %pack.2 = (f32[128,128]{1,0:T(8,128)S(1)}, f32[128,128]{1,0:T(8,128)S(1)}, f32[1,256,128]{2,1,0:T(8,128)S(1)}) custom-call(f32[1,256,128]{2,1,0:T(8,128)S(1)} %get-tuple-element.22.refs_0_, f32[1,256,128]{2,1,0:T(8,128)S(1)} %collective-permute-done.refs_1_, f32[1,256,128]{2,1,0:T(8,128)S(1)} %collective-permute-done.1.refs_2_, ...), custom_call_target="tpu_custom_call" | custom-call | tf_op jit(solution)/shard_map/pack/pallas_call | solution.py:412
  20.5 1.0 %collective-permute-done.3.refs_1_ = f32[1,256,128]{2,1,0:T(8,128)S(1)} collective-permute-done((f32[1,256,128]{2,1,0:T(8,128)S(1)}, f32[1,256,128]{2,1,0:T(8,128)S(1)}, u32[]{:S(2)}, u32[]{:S(2)}) %collective-permute-start.3) | collective-permute-done | bytes 131104 | tf_op jit(solution)/shard_map/ppermute | solution.py:522
  21.5 1.6 %collective-permute-done.4.refs_2_ = f32[1,256,128]{2,1,0:T(8,128)S(1)} collective-permute-done((f32[1,256,128]{2,1,0:T(8,128)S(1)}, f32[1,256,128]{2,1,0:T(8,128)S(1)}, u32[]{:S(2)}, u32[]{:S(2)}) %collective-permute-start.4) | collective-permute-done | bytes 131104 | tf_op jit(solution)/shard_map/ppermute | solution.py:522
  23.1 1.9 %collective-permute-done.5.refs_3_ = f32[1,256,128]{2,1,0:T(8,128)S(1)} collective-permute-done((f32[1,256,128]{2,1,0:T(8,128)S(1)}, f32[1,256,128]{2,1,0:T(8,128)S(1)}, u32[]{:S(2)}, u32[]{:S(2)}) %collective-permute-start.5) | collective-permute-done | bytes 131104 | tf_op jit(solution)/shard_map/ppermute | solution.py:522
  25.0 0.7 %pack.3 = (f32[136,128]{1,0:T(8,128)S(1)}, f32[136,128]{1,0:T(8,128)S(1)}) custom-call(f32[1,256,128]{2,1,0:T(8,128)S(1)} %get-tuple-element.30.refs_0_, f32[1,256,128]{2,1,0:T(8,128)S(1)} %collective-permute-done.3.refs_1_, f32[1,256,128]{2,1,0:T(8,128)S(1)} %collective-permute-done.4.refs_2_, f32[1,256,128]{2,1,0:T(8,128)S(1)} %collective-permute-done.5.refs_3_, ...), custom_call_target="tpu_custom_call" | custom-call | tf_op jit(solution)/shard_map/pack/pallas_call | solution.py:412
  25.7 2.9 %collective-permute-start.7 = (f32[136,128]{1,0:T(8,128)S(1)}, f32[136,128]{1,0:T(8,128)S(1)}, u32[]{:S(2)}, u32[]{:S(2)}) collective-permute-start(f32[136,128]{1,0:T(8,128)S(1)} %get-tuple-element.37), channel_id=1, source_target_pairs={{0,8},{2,10},{4,12},{6,14},{8,0},{10,2},{12,4},{14,6},{1,9},{3,11}... | collective-permute-start | bytes 208904 | tf_op jit(solution)/shard_map/ppermute | solution.py:522
  28.5 0.1 collective-permute-start.6
  28.6 5.8 %collective-permute-done.6.refs_2_ = f32[128,128]{1,0:T(8,128)S(1)} collective-permute-done((f32[128,128]{1,0:T(8,128)S(1)}, f32[128,128]{1,0:T(8,128)S(1)}, u32[]{:S(2)}, u32[]{:S(2)}) %collective-permute-start.6) | collective-permute-done | bytes 65568 | tf_op jit(solution)/shard_map/ppermute | solution.py:522
  34.4 0.3 finish.1
  34.7 1.0 %collective-permute-start.10 = (f32[40,128]{1,0:T(8,128)S(1)}, f32[40,128]{1,0:T(8,128)S(1)}, u32[]{:S(2)}, u32[]{:S(2)}) collective-permute-start(f32[40,128]{1,0:T(8,128)S(1)} %get-tuple-element.41), channel_id=1, source_target_pairs={{0,6},{2,4},{4,2},{6,0},{8,14},{10,12},{12,10},{14,8},{1,7},{3,5},... | collective-permute-start | bytes 61448 | tf_op jit(solution)/shard_map/ppermute | solution.py:522
  35.7 0.7 %collective-permute-start.8 = (f32[40,128]{1,0:T(8,128)S(1)}, f32[40,128]{1,0:T(8,128)S(1)}, u32[]{:S(2)}, u32[]{:S(2)}) collective-permute-start(f32[40,128]{1,0:T(8,128)S(1)} %get-tuple-element.39), channel_id=1, source_target_pairs={{0,2},{2,0},{4,6},{6,4},{8,10},{10,8},{12,14},{14,12},{1,3},{3,1},... | collective-permute-start | bytes 61448 | tf_op jit(solution)/shard_map/ppermute | solution.py:522
  36.5 1.8 %collective-permute-start.9 = (f32[40,128]{1,0:T(8,128)S(1)}, f32[40,128]{1,0:T(8,128)S(1)}, u32[]{:S(2)}, u32[]{:S(2)}) collective-permute-start(f32[40,128]{1,0:T(8,128)S(1)} %get-tuple-element.40), channel_id=1, source_target_pairs={{0,4},{2,6},{4,0},{6,2},{8,12},{10,14},{12,8},{14,10},{1,5},{3,7},... | collective-permute-start | bytes 61448 | tf_op jit(solution)/shard_map/ppermute | solution.py:522
  38.3 1.2 %collective-permute-done.10.refs_3_ = f32[40,128]{1,0:T(8,128)S(1)} collective-permute-done((f32[40,128]{1,0:T(8,128)S(1)}, f32[40,128]{1,0:T(8,128)S(1)}, u32[]{:S(2)}, u32[]{:S(2)}) %collective-permute-start.10) | collective-permute-done | bytes 20512 | tf_op jit(solution)/shard_map/ppermute | solution.py:522
  39.5 0.2 collective-permute-done.8.refs_1_
  39.7 0.6 %collective-permute-done.9.refs_2_ = f32[40,128]{1,0:T(8,128)S(1)} collective-permute-done((f32[40,128]{1,0:T(8,128)S(1)}, f32[40,128]{1,0:T(8,128)S(1)}, u32[]{:S(2)}, u32[]{:S(2)}) %collective-permute-start.9) | collective-permute-done | bytes 20512 | tf_op jit(solution)/shard_map/ppermute | solution.py:522
  40.3 0.6 %place_outputs.1 = (bf16[2,4,16,128]{3,2,1,0:T(8,128)(2,1)}, bf16[2,512]{1,0:T(2,128)(2,1)}) custom-call(f32[40,128]{1,0:T(8,128)S(1)} %get-tuple-element.38.refs_0_, f32[40,128]{1,0:T(8,128)S(1)} %collective-permute-done.8.refs_1_, f32[40,128]{1,0:T(8,128)S(1)} %collective-permute-done.9.refs_2_, f32[40,128]{1,0:T(8,128)S(1)} %collective-permute-done.10.refs_3_), custom_call_target="tpu_custom_call" | custom-call | tf_op jit(solution)/shard_map/place_outputs/pallas_call | solution.py:495
  (19 shorter events, 0.0 us)
Async XLA Ops:
  7.0 12.1 %collective-permute-start = (f32[1,256,128]{2,1,0:T(8,128)S(1)}, f32[1,256,128]{2,1,0:T(8,128)S(1)}, u32[]{:S(2)}, u32[]{:S(2)}) collective-permute-start(f32[1,256,128]{2,1,0:T(8,128)S(1)} %get-tuple-element.23), channel_id=1, source_target_pairs={{0,2},{2,0},{4,6},{6,4},{8,10},{10,8},{12,14},{14,12},{1,3},{3,1},... | collective-permute-start | bytes 393224 | tf_op jit(solution)/shard_map/ppermute | solution.py:522
  10.1 9.8 %collective-permute-start.1 = (f32[1,256,128]{2,1,0:T(8,128)S(1)}, f32[1,256,128]{2,1,0:T(8,128)S(1)}, u32[]{:S(2)}, u32[]{:S(2)}) collective-permute-start(f32[1,256,128]{2,1,0:T(8,128)S(1)} %get-tuple-element.24), channel_id=1, source_target_pairs={{0,4},{2,6},{4,0},{6,2},{8,12},{10,14},{12,8},{14,10},{1,5},{3,7},... | collective-permute-start | bytes 393224 | tf_op jit(solution)/shard_map/ppermute | solution.py:522
  11.7 8.3 %collective-permute-start.2 = (f32[1,256,128]{2,1,0:T(8,128)S(1)}, f32[1,256,128]{2,1,0:T(8,128)S(1)}, u32[]{:S(2)}, u32[]{:S(2)}) collective-permute-start(f32[1,256,128]{2,1,0:T(8,128)S(1)} %get-tuple-element.25), channel_id=1, source_target_pairs={{0,6},{2,4},{4,2},{6,0},{8,14},{10,12},{12,10},{14,8},{1,7},{3,5},... | collective-permute-start | bytes 393224 | tf_op jit(solution)/shard_map/ppermute | solution.py:522
  11.7 7.5 %copy-start = (bf16[2048,512]{1,0:T(8,128)(2,1)S(1)}, bf16[2048,512]{1,0:T(8,128)(2,1)}, u32[]{:S(2)}) copy-start(bf16[2048,512]{1,0:T(8,128)(2,1)} %refs_2_.3) | copy-start | bytes 6291460
  11.7 7.5 %copy-start.1 = (bf16[2048,8]{0,1:T(8,128)(2,1)S(1)}, bf16[2048,8]{0,1:T(8,128)(2,1)}, u32[]{:S(2)}) copy-start(bf16[2048,8]{0,1:T(8,128)(2,1)} %param.16) | copy-start | bytes 98308
  11.7 7.5 %copy-start.2 = (bf16[2048,8]{0,1:T(8,128)(2,1)S(1)}, bf16[2048,8]{0,1:T(8,128)(2,1)}, u32[]{:S(2)}) copy-start(bf16[2048,8]{0,1:T(8,128)(2,1)} %param.17) | copy-start | bytes 98308
  11.7 7.5 %copy-start.3 = (bf16[2,2048]{1,0:T(2,128)(2,1)S(1)}, bf16[2,2048]{1,0:T(2,128)(2,1)}, u32[]{:S(2)}) copy-start(bf16[2,2048]{1,0:T(2,128)(2,1)} %refs_0_.3) | copy-start | bytes 24580
  11.7 7.5 %copy-start.4 = (f32[4]{0:T(128)S(1)}, f32[4]{0:T(128)}, u32[]{:S(2)}) copy-start(f32[4]{0:T(128)} %param.18) | copy-start | bytes 52
  11.7 7.5 %copy-start.5 = (f32[4]{0:T(128)S(1)}, f32[4]{0:T(128)}, u32[]{:S(2)}) copy-start(f32[4]{0:T(128)} %param.19) | copy-start | bytes 52
  15.6 5.9 %collective-permute-start.3 = (f32[1,256,128]{2,1,0:T(8,128)S(1)}, f32[1,256,128]{2,1,0:T(8,128)S(1)}, u32[]{:S(2)}, u32[]{:S(2)}) collective-permute-start(f32[1,256,128]{2,1,0:T(8,128)S(1)} %get-tuple-element.31), channel_id=1, source_target_pairs={{0,2},{2,0},{4,6},{6,4},{8,10},{10,8},{12,14},{14,12},{1,3},{3,1},... | collective-permute-start | bytes 393224 | tf_op jit(solution)/shard_map/ppermute | solution.py:522
  17.5 5.5 %collective-permute-start.4 = (f32[1,256,128]{2,1,0:T(8,128)S(1)}, f32[1,256,128]{2,1,0:T(8,128)S(1)}, u32[]{:S(2)}, u32[]{:S(2)}) collective-permute-start(f32[1,256,128]{2,1,0:T(8,128)S(1)} %get-tuple-element.32), channel_id=1, source_target_pairs={{0,4},{2,6},{4,0},{6,2},{8,12},{10,14},{12,8},{14,10},{1,5},{3,7},... | collective-permute-start | bytes 393224 | tf_op jit(solution)/shard_map/ppermute | solution.py:522
  19.1 15.3 %copy-start.6 = (f32[128]{0:T(128)S(1)}, f32[128]{0:T(128)}, u32[]{:S(2)}) copy-start(f32[128]{0:T(128)} %param.23) | copy-start | bytes 1540
  19.1 5.9 %collective-permute-start.5 = (f32[1,256,128]{2,1,0:T(8,128)S(1)}, f32[1,256,128]{2,1,0:T(8,128)S(1)}, u32[]{:S(2)}, u32[]{:S(2)}) collective-permute-start(f32[1,256,128]{2,1,0:T(8,128)S(1)} %get-tuple-element.33), channel_id=1, source_target_pairs={{0,6},{2,4},{4,2},{6,0},{8,14},{10,12},{12,10},{14,8},{1,7},{3,5},... | collective-permute-start | bytes 393224 | tf_op jit(solution)/shard_map/ppermute | solution.py:522
  25.7 8.7 %collective-permute-start.7 = (f32[136,128]{1,0:T(8,128)S(1)}, f32[136,128]{1,0:T(8,128)S(1)}, u32[]{:S(2)}, u32[]{:S(2)}) collective-permute-start(f32[136,128]{1,0:T(8,128)S(1)} %get-tuple-element.37), channel_id=1, source_target_pairs={{0,8},{2,10},{4,12},{6,14},{8,0},{10,2},{12,4},{14,6},{1,9},{3,11}... | collective-permute-start | bytes 208904 | tf_op jit(solution)/shard_map/ppermute | solution.py:522
  28.5 5.9 %collective-permute-start.6 = (f32[128,128]{1,0:T(8,128)S(1)}, f32[128,128]{1,0:T(8,128)S(1)}, u32[]{:S(2)}, u32[]{:S(2)}) collective-permute-start(f32[128,128]{1,0:T(8,128)S(1)} %get-tuple-element.36), channel_id=1, source_target_pairs={{0,8},{2,10},{4,12},{6,14},{8,0},{10,2},{12,4},{14,6},{1,9},{3,11}... | collective-permute-start | bytes 196616 | tf_op jit(solution)/shard_map/ppermute | solution.py:522
  34.7 4.7 %collective-permute-start.10 = (f32[40,128]{1,0:T(8,128)S(1)}, f32[40,128]{1,0:T(8,128)S(1)}, u32[]{:S(2)}, u32[]{:S(2)}) collective-permute-start(f32[40,128]{1,0:T(8,128)S(1)} %get-tuple-element.41), channel_id=1, source_target_pairs={{0,6},{2,4},{4,2},{6,0},{8,14},{10,12},{12,10},{14,8},{1,7},{3,5},... | collective-permute-start | bytes 61448 | tf_op jit(solution)/shard_map/ppermute | solution.py:522
  35.7 3.9 %collective-permute-start.8 = (f32[40,128]{1,0:T(8,128)S(1)}, f32[40,128]{1,0:T(8,128)S(1)}, u32[]{:S(2)}, u32[]{:S(2)}) collective-permute-start(f32[40,128]{1,0:T(8,128)S(1)} %get-tuple-element.39), channel_id=1, source_target_pairs={{0,2},{2,0},{4,6},{6,4},{8,10},{10,8},{12,14},{14,12},{1,3},{3,1},... | collective-permute-start | bytes 61448 | tf_op jit(solution)/shard_map/ppermute | solution.py:522
  36.5 3.8 %collective-permute-start.9 = (f32[40,128]{1,0:T(8,128)S(1)}, f32[40,128]{1,0:T(8,128)S(1)}, u32[]{:S(2)}, u32[]{:S(2)}) collective-permute-start(f32[40,128]{1,0:T(8,128)S(1)} %get-tuple-element.40), channel_id=1, source_target_pairs={{0,4},{2,6},{4,0},{6,2},{8,12},{10,14},{12,8},{14,10},{1,5},{3,7},... | collective-permute-start | bytes 61448 | tf_op jit(solution)/shard_map/ppermute | solution.py:522
